TPU v7x, 128 devices: a whole 4x4x4 slice. The times are simulated.
128 devices in a mesh: ep: 32 (over z, y, core), tp: 4 (over x).
Axes of the slice: x: 4, y: 4, z: 4, core: 2. Of those that a mesh axis runs over, the one named last changes fastest.
Arguments:
- tokens: bfloat16 [1536, 2048], P('ep'), may hold values from -6 to 6
- mix_gain: float32 [2048], replicated, may hold values from 0.1 to 1.9
- w_query: bfloat16 [2048, 1024], P(None, 'tp'), may hold values from -0.125 to 0.125
- w_key: bfloat16 [2048, 1024], P(None, 'tp'), may hold values from -0.125 to 0.125
- w_value: bfloat16 [2048, 1024], P(None, 'tp'), may hold values from -0.125 to 0.125
- w_outgate: bfloat16 [2048, 1024], P(None, 'tp'), may hold values from -0.125 to 0.125
- w_ingate: bfloat16 [2048, 8], P(None, 'tp'), may hold values from -0.125 to 0.125
- w_forget: bfloat16 [2048, 8], P(None, 'tp'), may hold values from -0.125 to 0.125
- in_bias: float32 [8], P('tp'), may hold values from -2 to 1
- forget_bias: float32 [8], P('tp'), may hold values from -1 to 4
- w_mix_out: bfloat16 [1024, 2048], replicated, may hold values from -0.1875 to 0.1875
- cell_state: float32 [1536, 8, 128, 128], P('ep', 'tp'), may hold values from -0.5 to 0.5
- norm_state: float32 [1536, 8, 128], P('ep', 'tp'), may hold values from -0.5 to 0.5
- max_state: float32 [1536, 8], P('ep', 'tp'), may hold values from -1 to 2
- moe_gain: float32 [2048], replicated, may hold values from 0.1 to 1.9
- route_ids: int32 [1536, 2], P('ep'), may hold values from 0 to 31, as said below
- route_weights: float32 [1536, 2], P('ep'), may hold values from 0.2 to 1
- expert_gate: bfloat16 [32, 2048, 1024], P('ep', None, 'tp'), may hold values from -0.125 to 0.125
- expert_up: bfloat16 [32, 2048, 1024], P('ep', None, 'tp'), may hold values from -0.125 to 0.125
- expert_down: bfloat16 [32, 1024, 2048], P('ep', 'tp'), may hold values from -0.1875 to 0.1875
- branch_gate: bfloat16 [2048], replicated, may hold values from -0.125 to 0.125
- dense_gate: bfloat16 [2048, 8192], P(None, ('ep', 'tp')), may hold values from -0.125 to 0.125
- dense_up: bfloat16 [2048, 8192], P(None, ('ep', 'tp')), may hold values from -0.125 to 0.125
- dense_down: bfloat16 [8192, 2048], P(('ep', 'tp')), may hold values from -0.25 to 0.25
Outputs:
- layer_out: bfloat16 [1536, 2048], P('ep', 'tp')
- new_cell: float32 [1536, 8, 128, 128], P('ep', 'tp')
- new_norm: float32 [1536, 8, 128], P('ep', 'tp')
- new_max: float32 [1536, 8], P('ep', 'tp')
Inputs may be any that keep to these rules, and one draw needn't show every extreme that they name: `route_ids`: each row names two different experts of one group of 8 consecutive ids. Within the rows of one device no id appears more than 6 times, and some id appears exactly 6 times.
All inputs are finite; a program needn't handle non-finite values.
Results may differ from a plain program's by a relative error of at most 0.009.
The roundings to bfloat16 on the way count: a program that leaves them out, or rounds other values in their place, can miss the bound.
Values may be sent and summed in bfloat16 or wider, within the bound.
A program may use at most 128 MiB of HBM per device.

v0:
```python
import jax
import jax.numpy as jnp
from jax import lax
from jax.sharding import PartitionSpec as P

EPS = 1e-06


def in_order(parts, dim):
    parts = jnp.moveaxis(parts, 0, dim)
    dims = parts.shape
    return parts.reshape(*dims[:dim], dims[dim] * dims[dim + 1], *dims[dim + 2 :])


def sent_to_all(array, axis):
    copies = jnp.broadcast_to(array, (lax.axis_size(axis), *array.shape))
    return lax.all_to_all(copies, axis, split_axis=0, concat_axis=0, tiled=True)


def collect(array, axis, dim):
    return in_order(sent_to_all(array, axis), dim)


def turned_gather(arrays, axis, dims):
    turned = [jnp.moveaxis(a, dim, 0) for a, dim in zip(arrays, dims)]
    both = jnp.concatenate([t.reshape(len(t), -1) for t in turned], axis=1)
    filled, at, done = (lax.all_gather(both, axis, axis=0, tiled=True), 0, [])
    for t, dim in zip(turned, dims):
        piece = filled[:, at : at + t[0].size].reshape(-1, *t.shape[1:])
        done.append(jnp.moveaxis(piece, 0, dim))
        at += t[0].size
    return tuple(done)


def split_up(array, dim, size):
    dims = array.shape
    parts = array.reshape(*dims[:dim], size, dims[dim] // size, *dims[dim + 1 :])
    return jnp.moveaxis(parts, dim, 0)


def summed_on_arrival(array, axis, dim):
    parts = split_up(array, dim, lax.axis_size(axis))
    arrived = lax.all_to_all(parts, axis, split_axis=0, concat_axis=0, tiled=True)
    return arrived.astype(jnp.float32).sum(axis=0)


def norm_rows(rows_in, gain_vec):
    as_float = rows_in.astype(jnp.float32)
    scaled = as_float * lax.rsqrt(jnp.mean(as_float * as_float, axis=-1, keepdims=True) + EPS)
    return (scaled * gain_vec).astype(jnp.bfloat16)


def swiglu(tok_rows, gate_w, up_w):
    gate_proj = jnp.dot(tok_rows, gate_w, preferred_element_type=jnp.float32)
    up_proj = jnp.dot(tok_rows, up_w, preferred_element_type=jnp.float32)
    return (jax.nn.silu(gate_proj) * up_proj).astype(jnp.bfloat16)


def branch_weight(tok_rows, branch_gate):
    return jax.nn.sigmoid(jnp.dot(tok_rows, branch_gate, preferred_element_type=jnp.float32))


def cell_step(
    normed,
    w_query,
    w_key,
    w_value,
    w_outgate,
    w_ingate,
    w_forget,
    in_bias,
    forget_bias,
    cell_state,
    norm_state,
    max_state,
):
    row_count, head_count = max_state.shape
    head_size = cell_state.shape[2]

    def project(weight):
        return jnp.dot(normed, weight, preferred_element_type=jnp.float32)

    queries = project(w_query).reshape(row_count, head_count, head_size)
    key_vecs = project(w_key).reshape(row_count, head_count, head_size) * head_size ** (-0.5)
    values = project(w_value).reshape(row_count, head_count, head_size)
    outgate = project(w_outgate)
    in_pre = project(w_ingate) + in_bias
    log_forget = jax.nn.log_sigmoid(project(w_forget) + forget_bias)
    new_max = jnp.maximum(log_forget + max_state, in_pre)
    carry_factor = jnp.exp(log_forget + max_state - new_max)
    write_factor = jnp.exp(in_pre - new_max)
    written = write_factor[..., None] * key_vecs
    new_cell = (
        carry_factor[..., None, None] * cell_state + written[..., :, None] * values[..., None, :]
    )
    new_norm = carry_factor[..., None] * norm_state + written
    numerator = jnp.einsum("bhd,bhde->bhe", queries, new_cell, precision=lax.Precision.HIGHEST)
    denominator = jnp.sum(queries * new_norm, axis=-1)
    cell_out = numerator / jnp.maximum(jnp.abs(denominator), jnp.exp(-new_max))[..., None]
    mixed_heads = (
        jax.nn.sigmoid(outgate) * cell_out.reshape(row_count, head_count * head_size)
    ).astype(jnp.bfloat16)
    return (mixed_heads, new_cell, new_norm, new_max)


def local(
    tokens,
    mix_gain,
    w_query,
    w_key,
    w_value,
    w_outgate,
    w_ingate,
    w_forget,
    in_bias,
    forget_bias,
    w_mix_out,
    cell_state,
    norm_state,
    max_state,
    moe_gain,
    route_ids,
    route_weights,
    expert_gate,
    expert_up,
    expert_down,
    branch_gate,
    dense_gate,
    dense_up,
    dense_down,
):
    seq_dev, model_width = tokens.shape
    tp_count = lax.axis_size("tp")
    ep_count = lax.axis_size("ep")
    col_width = model_width // tp_count
    normed = norm_rows(tokens, mix_gain)
    mixed_heads, new_cell, new_norm, new_max = cell_step(
        normed,
        w_query,
        w_key,
        w_value,
        w_outgate,
        w_ingate,
        w_forget,
        in_bias,
        forget_bias,
        cell_state,
        norm_state,
        max_state,
    )
    all_heads = collect(mixed_heads, "tp", 1)
    mixed_proj = jnp.dot(all_heads, w_mix_out, preferred_element_type=jnp.float32)
    residual = (tokens.astype(jnp.float32) + mixed_proj).astype(jnp.bfloat16)
    moe_in = norm_rows(residual, moe_gain)
    gathered = lax.all_gather(moe_in, "ep", axis=0, tiled=True)
    gate_block, up_block = turned_gather((dense_gate, dense_up), "tp", (1, 1))
    down_block = lax.all_to_all(dense_down, "tp", split_axis=1, concat_axis=0, tiled=True)
    hidden = swiglu(gathered, gate_block, up_block)
    partial_value = jnp.dot(hidden, down_block, preferred_element_type=jnp.float32)
    dense_out = summed_on_arrival(
        (partial_value * branch_weight(gathered, branch_gate)[:, None]).astype(jnp.bfloat16),
        "ep",
        0,
    )
    local_experts = expert_gate.shape[0]
    experts = ep_count * local_experts
    capacity = max(2, 4 * seq_dev // experts)
    top_count = route_ids.shape[1]
    flat_ids = route_ids.reshape(-1)
    position = jnp.arange(flat_ids.shape[0], dtype=jnp.int32)
    earlier = (flat_ids[:, None] == flat_ids[None, :]) & (position[None, :] < position[:, None])
    slot_rank = jnp.sum(earlier.astype(jnp.int32), axis=1)
    slot_index = flat_ids * capacity + slot_rank
    owner_row = position // top_count
    slots_all = jnp.arange(experts * capacity, dtype=jnp.int32)
    matches = slots_all[:, None] == slot_index[None, :]
    source_row = jnp.sum(jnp.where(matches, owner_row[None, :] + 1, 0), axis=1) - 1
    source_row = jnp.where(source_row < 0, seq_dev, source_row)
    padded = jnp.concatenate([moe_in, jnp.zeros((1, model_width), jnp.bfloat16)], axis=0)
    dispatch = jnp.take(padded, source_row, axis=0).reshape(
        ep_count, local_experts, capacity, model_width
    )
    received = lax.all_to_all(dispatch, "ep", split_axis=0, concat_axis=0, tiled=True)
    gate_proj = jnp.einsum(
        "secd,edf->secf", received, expert_gate, preferred_element_type=jnp.float32
    )
    up_proj = jnp.einsum("secd,edf->secf", received, expert_up, preferred_element_type=jnp.float32)
    hidden = (jax.nn.silu(gate_proj) * up_proj).astype(jnp.bfloat16)
    full_out = jnp.einsum("secf,efd->secd", hidden, expert_down, preferred_element_type=jnp.float32)
    summed = summed_on_arrival(full_out.astype(jnp.bfloat16), "tp", 3)
    returned = lax.all_to_all(
        summed.astype(jnp.bfloat16), "ep", split_axis=0, concat_axis=0, tiled=True
    ).astype(summed.dtype)
    returned = returned.reshape(experts * capacity, col_width)
    picked = jnp.take(returned, slot_index, axis=0) * route_weights.reshape(-1)[:, None]
    moe_out = jnp.sum(picked.reshape(seq_dev, top_count, col_width), axis=1)
    own_cols = lax.dynamic_slice_in_dim(
        residual, lax.axis_index("tp") * col_width, col_width, 1
    ).astype(jnp.float32)
    layer_out = (own_cols + moe_out + dense_out).astype(jnp.bfloat16)
    return (layer_out, new_cell, new_norm, new_max)


def solution(mesh):
    in_specs = (
        P("ep", None),
        P(),
        P(None, "tp"),
        P(None, "tp"),
        P(None, "tp"),
        P(None, "tp"),
        P(None, "tp"),
        P(None, "tp"),
        P("tp"),
        P("tp"),
        P(),
        P("ep", "tp", None, None),
        P("ep", "tp", None),
        P("ep", "tp"),
        P(),
        P("ep", None),
        P("ep", None),
        P("ep", None, "tp"),
        P("ep", None, "tp"),
        P("ep", "tp", None),
        P(),
        P(None, ("ep", "tp")),
        P(None, ("ep", "tp")),
        P(("ep", "tp"), None),
    )
    out_specs = (P("ep", "tp"), P("ep", "tp", None, None), P("ep", "tp", None), P("ep", "tp"))
    return jax.shard_map(local, mesh=mesh, in_specs=in_specs, out_specs=out_specs, check_vma=False)
```

profile of v0, /device:TPU:1, one launch (start us, length us, event | category | flops | bytes accessed | tf_op | source)
XLA Modules:
  0.0 159.3 jit_solution(14502547936491669466)
XLA Ops:
  7.3 2.0 %pad_maximum_fusion = bf16[64,4096]{1,0:T(8,128)(2,1)} fusion(bf16[64,2048]{1,0:T(8,128)(2,1)} %bitcast.109, bf16[64,2048]{1,0:T(8,128)(2,1)} %bitcast.110), kind=kLoop, calls=%fused_computation.41 | loop fusion | flops 1048576 | bytes 1048576 | tf_op jit(solution)/shard_map/concatenate | solution.py:26
  9.4 1.1 fusion.32
  10.4 1.7 %fusion.54 = f32[48,256]{1,0:T(8,128)S(1)} fusion(bf16[2048,256]{1,0:T(8,128)(2,1)} %param.26, bf16[48,2048]{1,0:T(8,128)(2,1)} %param.24, f32[2048]{0:T(1024)} %param.25, f32[48]{0:T(128)S(1)} %add_rsqrt_fusion.1), kind=kOutput, calls=%fused_computation.101 | convolution fusion | flops 50724864 | bytes 1302720 | tf_op jit(solution)/shard_map/dot_general | solution.py:81
  12.8 1.2 convolution_add_fusion.1
  14.0 1.2 subtract_exponential_fusion
  15.3 0.7 copy.85
  16.1 1.0 fusion.50
  17.5 1.6 %multiply_reduce_fusion.1 = (f32[48,2]{1,0:T(8,128)S(1)}, f32[48,2,128]{2,1,0:T(2,128)}, f32[48,2,128]{2,1,0:T(2,128)S(1)}) fusion(f32[48,2,128]{2,1,0:T(2,128)} %reshape.212, f32[48,2,128]{2,1,0:T(2,128)} %param.36, f32[48,2]{1,0:T(8,128)S(1)} %copy.84, f32[48,2,128]{2,1,0:T(2,128)S(1)} %reshape.213, f32[48,2]{1,0:T(8,128)} %copy.85), kind=kLoop, calls=%fused_computation.63 | loop fusion | flops 61344 | bytes 246912 | tf_op jit(solution)/shard_map/reduce_sum | solution.py:98
  19.3 4.7 %multiply_add_fusion = f32[48,2,128,128]{3,2,1,0:T(8,128)S(1)} fusion(f32[48,2,128,128]{3,2,1,0:T(8,128)} %param.35, f32[48,2,128]{2,1,0:T(2,128)S(1)} %mul.166, f32[48,2,128]{2,1,0:T(2,128)S(1)} %get-tuple-element.6, f32[48,2]{1,0:T(8,128)S(1)} %copy.84), kind=kLoop, calls=%fused_computation.2 | loop fusion | flops 4718592 | bytes 12681600 | tf_op jit(solution)/shard_map/add | solution.py:94
  24.1 5.5 %fusion.57 = f32[48,2,1,128]{3,2,1,0:T(1,128)S(1)} fusion(f32[48,2,128,1]{2,3,1,0:T(1,128)S(1)} %bitcast.111, f32[48,2,128,128]{3,2,1,0:T(8,128)S(1)} %multiply_add_fusion), kind=kOutput, calls=%fused_computation.102 | convolution fusion | flops 18874368 | bytes 6389760 | tf_op jit(solution)/shard_map/bhd,bhde->bhe/dot_general | solution.py:97
  30.0 10.6 %all_to_all.44 = bf16[4,48,256]{2,1,0:T(8,128)(2,1)S(1)} all-to-all(bf16[4,48,256]{2,1,0:T(8,128)(2,1)S(1)} %broadcast_in_dim.37), channel_id=1, replica_groups=mesh['ep'=32,'tp'=4] {'tp'}, dimensions={0} | all-to-all | bytes 196608 | tf_op jit(solution)/shard_map/all_to_all | solution.py:17
  40.6 1.0 fusion.29
  41.6 0.8 fusion.31
  43.2 0.9 concatenate.6
  44.1 1.1 gather_fusion
  45.7 29.8 %all_to_all.45 = bf16[32,1,6,2048]{3,2,1,0:T(8,128)(2,1)S(1)} all-to-all(bf16[32,1,6,2048]{3,2,1,0:T(8,128)(2,1)S(1)} %select_bitcast_fusion), channel_id=1, replica_groups=mesh['ep'=32,'tp'=4] {'ep'}, dimensions={0} | all-to-all | bytes 1572864 | tf_op jit(solution)/shard_map/all_to_all | solution.py:183
  76.3 2.3 %convolution_convert_fusion = bf16[32,6,2048]{2,0,1:T(8,128)(2,1)S(1)} fusion(bf16[1,256,2048]{2,1,0:T(8,128)(2,1)S(1)} %copy-done, bf16[1,2048,256]{2,1,0:T(8,128)(2,1)} %param.42, bf16[32,1,6,2048]{3,2,1,0:T(8,128)(2,1)S(1)} %all_to_all.45, f32[32,1,6,256]{3,0,2,1:T(8,128)S(1)} %convolution_bitcast_fusion.1), kind=kOutput, calls=%fused_computation.8 | convolution fusion | flops 403341312 | bytes 3866624 | tf_op jit(solution)/shard_map/secf,efd->secd/dot_general | solution.py:189
  78.6 1.0 copy.120
  79.6 3.5 %all-to-all-start.2 = ((bf16[4,32,1,6,512]{4,1,3,2,0:T(8,128)(2,1)}), bf16[4,32,1,6,512]{4,1,3,2,0:T(8,128)(2,1)S(1)}, u32[]{:S(2)}, u32[]{:S(2)}) async-start(bf16[4,32,1,6,512]{4,1,3,2,0:T(8,128)(2,1)} %bitcast.100), calls=%async_computation.2 | async-start | bytes 1572864 | tf_op jit(solution)/shard_map/all_to_all | solution.py:43
  83.1 0.7 copy.121
  83.8 11.3 %all-to-all-done.2 = bf16[4,32,1,6,512]{4,1,3,2,0:T(8,128)(2,1)S(1)} async-done(((bf16[4,32,1,6,512]{4,1,3,2,0:T(8,128)(2,1)}), bf16[4,32,1,6,512]{4,1,3,2,0:T(8,128)(2,1)S(1)}, u32[]{:S(2)}, u32[]{:S(2)}) %all-to-all-start.2) | async-done | bytes 786464 | tf_op jit(solution)/shard_map/all_to_all | solution.py:43
  95.2 3.6 %all-to-all-start.4 = ((bf16[64,4,512]{2,0,1:T(8,128)(2,1)}), bf16[64,4,512]{2,0,1:T(8,128)(2,1)S(1)}, u32[]{:S(2)}, u32[]{:S(2)}) async-start(bf16[64,4,512]{2,0,1:T(8,128)(2,1)} %bitcast.101), calls=%async_computation.4 | async-start | bytes 524288 | tf_op jit(solution)/shard_map/all_to_all | solution.py:157
  98.9 0.8 copy.97
  99.7 2.0 %all-gather.3.cloned.1.call-done = bf16[1536,2048]{1,0:T(8,128)(2,1)} async-done(((bf16[48,2048]{1,0:T(8,128)(2,1)}), bf16[1536,2048]{1,0:T(8,128)(2,1)}) %all-gather.3.cloned.1.call-update) | async-done | bytes 6291472 | tf_op jit(solution)/shard_map/all_gather | solution.py:155
  101.8 6.2 %fusion.14 = f32[1536,256]{1,0:T(8,128)} fusion(bf16[1536,2048]{1,0:T(8,128)(2,1)} %all-gather.3.cloned.1.call-done, bf16[256,4096]{1,0:T(8,128)(2,1)} %all-gather.5.cloned.1.call-done), kind=kOutput, calls=%fused_computation.27 | convolution fusion | flops 1610612736 | bytes 8912896 | tf_op jit(solution)/shard_map/dot_general | solution.py:54
  108.0 1.7 %convolution_reduce_fusion = f32[1536]{0:T(1024)S(1)} fusion(bf16[1536,2048]{1,0:T(8,128)(2,1)S(1)} %copy-done.2, bf16[2048,1]{0,1:T(2,128)(2,1)S(1)} %reshape.249), kind=kOutput, calls=%fused_computation.22 | convolution fusion | flops 6291456 | bytes 6301696 | tf_op jit(solution)/shard_map/dot_general | solution.py:60
  109.8 4.7 %all-to-all-start.3 = ((bf16[32,1,6,512]{3,2,1,0:T(8,128)(2,1)}), bf16[32,1,6,512]{3,2,1,0:T(8,128)(2,1)S(1)}, u32[]{:S(2)}, u32[]{:S(2)}) async-start(bf16[32,1,6,512]{3,2,1,0:T(8,128)(2,1)} %copy.97), calls=%async_computation.3 | async-start | bytes 524288 | tf_op jit(solution)/shard_map/all_to_all | solution.py:191
  114.5 7.5 %fusion = bf16[1536,512]{1,0:T(8,128)(2,1)} fusion(bf16[256,512]{1,0:T(8,128)(2,1)S(1)} %bitcast.108, f32[1536]{0:T(1024)S(1)} %add_divide_fusion, bf16[1536,2048]{1,0:T(8,128)(2,1)} %all-gather.3.cloned.1.call-done, f32[1536,256]{1,0:T(8,128)} %fusion.14, bf16[256,4096]{1,0:T(8,128)(2,1)} %all-gather.5.cloned.1.call-done), kind=kOutput, calls=%fused_computation.5 | convolution fusion | flops 2017198080 | bytes 10754048 | tf_op jit(solution)/shard_map/dot_general | solution.py:159
  122.0 1.3 all-to-all-done.3
  123.4 6.0 %all-to-all-start.5 = ((bf16[32,48,512]{2,1,0:T(8,128)(2,1)}), bf16[32,48,512]{2,1,0:T(8,128)(2,1)S(1)}, u32[]{:S(2)}, u32[]{:S(2)}) async-start(bf16[32,48,512]{2,1,0:T(8,128)(2,1)} %bitcast.102), calls=%async_computation.5 | async-start | bytes 3145728 | tf_op jit(solution)/shard_map/all_to_all | solution.py:43
  130.2 0.7 gather_fusion.1
  131.3 20.3 %all-to-all-done.5 = bf16[32,48,512]{2,1,0:T(8,128)(2,1)S(1)} async-done(((bf16[32,48,512]{2,1,0:T(8,128)(2,1)}), bf16[32,48,512]{2,1,0:T(8,128)(2,1)S(1)}, u32[]{:S(2)}, u32[]{:S(2)}) %all-to-all-start.5) | async-done | bytes 1572896 | tf_op jit(solution)/shard_map/all_to_all | solution.py:43
  (85 shorter events, 6.0 us)
Async XLA Ops:
  7.2 69.1 %copy-start = (bf16[1,256,2048]{2,1,0:T(8,128)(2,1)S(1)}, bf16[1,256,2048]{2,1,0:T(8,128)(2,1)}, u32[]{:S(2)}) copy-start(bf16[1,256,2048]{2,1,0:T(8,128)(2,1)} %param.43) | copy-start | bytes 3145732
  7.2 8.9 %copy-start.3 = (bf16[48,2048]{1,0:T(8,128)(2,1)S(1)}, bf16[48,2048]{1,0:T(8,128)(2,1)}, u32[]{:S(2)}) copy-start(bf16[48,2048]{1,0:T(8,128)(2,1)} %param.24) | copy-start | bytes 589828
  7.2 9.9 %copy-start.9 = (f32[2048]{0:T(1024)S(1)}, f32[2048]{0:T(1024)}, u32[]{:S(2)}) copy-start(f32[2048]{0:T(1024)} %param.25) | copy-start | bytes 24580
  7.2 8.9 %copy-start.5 = (bf16[2048,256]{1,0:T(8,128)(2,1)S(1)}, bf16[2048,256]{1,0:T(8,128)(2,1)}, u32[]{:S(2)}) copy-start(bf16[2048,256]{1,0:T(8,128)(2,1)} %param.27) | copy-start | bytes 3145732
  7.2 9.9 %copy-start.6 = (bf16[2048,256]{1,0:T(8,128)(2,1)S(1)}, bf16[2048,256]{1,0:T(8,128)(2,1)}, u32[]{:S(2)}) copy-start(bf16[2048,256]{1,0:T(8,128)(2,1)} %param.28) | copy-start | bytes 3145732
  7.2 92.5 %all-gather.5.cloned.1.call-start = ((), (), s32[]{:S(2)}) async-start(), calls=%async_computation.7 | async-start | bytes 2621440 | tf_op jit(solution)/shard_map/all_gather | solution.py:27
  9.3 92.5 %all-gather.3.cloned.1.call-start = ((), (), s32[]{:S(2)}) async-start(), calls=%async_computation.6 | async-start | bytes 6488064 | tf_op jit(solution)/shard_map/all_gather | solution.py:155
  15.2 8.8 %copy-start.13 = (f32[48,2]{0,1:T(2,128)}, f32[48,2]{0,1:T(2,128)S(1)}, u32[]{:S(2)}) copy-start(f32[48,2]{0,1:T(2,128)S(1)} %get-tuple-element.8) | copy-start | bytes 1156
  24.0 17.6 %copy-start.1 = (f32[48,2,128,128]{3,2,1,0:T(8,128)}, f32[48,2,128,128]{3,2,1,0:T(8,128)S(1)}, u32[]{:S(2)}) copy-start(f32[48,2,128,128]{3,2,1,0:T(8,128)S(1)} %multiply_add_fusion) | copy-start | bytes 18874372
  24.0 5.6 %copy-start.7 = (bf16[2048,256]{1,0:T(8,128)(2,1)S(1)}, bf16[2048,256]{1,0:T(8,128)(2,1)}, u32[]{:S(2)}) copy-start(bf16[2048,256]{1,0:T(8,128)(2,1)} %param.29) | copy-start | bytes 3145732
  24.0 16.6 %copy-start.4 = (bf16[1024,2048]{1,0:T(8,128)(2,1)S(1)}, bf16[1024,2048]{1,0:T(8,128)(2,1)}, u32[]{:S(2)}) copy-start(bf16[1024,2048]{1,0:T(8,128)(2,1)} %param.34) | copy-start | bytes 12582916
  29.5 12.1 %copy-start.11 = (f32[2048]{0:T(1024)S(1)}, f32[2048]{0:T(1024)}, u32[]{:S(2)}) copy-start(f32[2048]{0:T(1024)} %param.38) | copy-start | bytes 24580
  29.5 12.9 %copy-start.10 = (s32[48,2]{0,1:T(2,128)S(1)}, s32[48,2]{0,1:T(2,128)}, u32[]{:S(2)}) copy-start(s32[48,2]{0,1:T(2,128)} %param.39) | copy-start | bytes 1156
  45.5 30.0 %copy-start.15 = (bf16[1,2048,256]{2,1,0:T(8,128)(2,1)S(1)}, bf16[1,2048,256]{2,1,0:T(8,128)(2,1)}, u32[]{:S(2)}) copy-start(bf16[1,2048,256]{2,1,0:T(8,128)(2,1)} %param.41) | copy-start | bytes 3145732
  75.6 7.5 %copy-start.12 = (bf16[2048]{0:T(1024)(128)(2,1)S(1)}, bf16[2048]{0:T(1024)(128)(2,1)}, u32[]{:S(2)}) copy-start(bf16[2048]{0:T(1024)(128)(2,1)} %param.44) | copy-start | bytes 12292
  75.6 7.6 %copy-start.8 = (bf16[64,2048]{1,0:T(8,128)(2,1)S(1)}, bf16[64,2048]{1,0:T(8,128)(2,1)}, u32[]{:S(2)}) copy-start(bf16[64,2048]{1,0:T(8,128)(2,1)} %param.47) | copy-start | bytes 786436
  79.6 15.6 %all-to-all-start.2 = ((bf16[4,32,1,6,512]{4,1,3,2,0:T(8,128)(2,1)}), bf16[4,32,1,6,512]{4,1,3,2,0:T(8,128)(2,1)S(1)}, u32[]{:S(2)}, u32[]{:S(2)}) async-start(bf16[4,32,1,6,512]{4,1,3,2,0:T(8,128)(2,1)} %bitcast.100), calls=%async_computation.2 | async-start | bytes 1572864 | tf_op jit(solution)/shard_map/all_to_all | solution.py:43
  95.2 14.6 %all-to-all-start.4 = ((bf16[64,4,512]{2,0,1:T(8,128)(2,1)}), bf16[64,4,512]{2,0,1:T(8,128)(2,1)S(1)}, u32[]{:S(2)}, u32[]{:S(2)}) async-start(bf16[64,4,512]{2,0,1:T(8,128)(2,1)} %bitcast.101), calls=%async_computation.4 | async-start | bytes 524288 | tf_op jit(solution)/shard_map/all_to_all | solution.py:157
  101.8 6.2 %copy-start.2 = (bf16[1536,2048]{1,0:T(8,128)(2,1)S(1)}, bf16[1536,2048]{1,0:T(8,128)(2,1)}, u32[]{:S(2)}) copy-start(bf16[1536,2048]{1,0:T(8,128)(2,1)} %all-gather.3.cloned.1.call-done) | copy-start | bytes 18874372
  109.8 13.6 %all-to-all-start.3 = ((bf16[32,1,6,512]{3,2,1,0:T(8,128)(2,1)}), bf16[32,1,6,512]{3,2,1,0:T(8,128)(2,1)S(1)}, u32[]{:S(2)}, u32[]{:S(2)}) async-start(bf16[32,1,6,512]{3,2,1,0:T(8,128)(2,1)} %copy.97), calls=%async_computation.3 | async-start | bytes 524288 | tf_op jit(solution)/shard_map/all_to_all | solution.py:191
  114.5 15.5 %copy-start.14 = (f32[48,2]{0,1:T(2,128)S(1)}, f32[48,2]{0,1:T(2,128)}, u32[]{:S(2)}) copy-start(f32[48,2]{0,1:T(2,128)} %param.40) | copy-start | bytes 1156
  123.4 28.2 %all-to-all-start.5 = ((bf16[32,48,512]{2,1,0:T(8,128)(2,1)}), bf16[32,48,512]{2,1,0:T(8,128)(2,1)S(1)}, u32[]{:S(2)}, u32[]{:S(2)}) async-start(bf16[32,48,512]{2,1,0:T(8,128)(2,1)} %bitcast.102), calls=%async_computation.5 | async-start | bytes 3145728 | tf_op jit(solution)/shard_map/all_to_all | solution.py:43
Sparse Core Ops, SparseCore 0:
  9.7 34.8 all-gather.4
  46.8 54.9 all-gather.2
where the time goes:
time: 161 us; the launch traced here: 159 us
  blocking collectives  40.4 us (25%)
  waiting for transfers between devices  35 us (22%)
  matrix products  30.7 us (19%)
  starting transfers between devices  17.9 us (11%)
  between operations  14.6 us (9%)
  other arithmetic  12.2 us (8%)
  local copies, waits for them, and re-layouts  8.5 us (5%)
    all_to_all x2, waiting for transfers between devices, summed_on_arrival(): lax.all_to_all(parts, axis, split_axis=0, concat_axis=0, tiled=True)  31.6 us
    all_to_all x1, blocking collectives, local(): lax.all_to_all(dispatch, 'ep', split_axis=0, concat_axis=0, tiled=True)  29.8 us
    all_to_all x1, blocking collectives, sent_to_all(): return lax.all_to_all(copies, axis, split_axis=0, concat_axis=0, tiled=True)  10.6 us
    all_to_all x2, starting transfers between devices, summed_on_arrival(): lax.all_to_all(parts, axis, split_axis=0, concat_axis=0, tiled=True)  9.53 us
    dot_general x1, matrix products, local(): jnp.dot(hidden, down_block, preferred_element_type=jnp.float32)  7.52 us
    dot_general x1, matrix products, swiglu(): gate_proj = jnp.dot(tok_rows, gate_w, preferred_element_type=jnp.float32)  6.24 us
    dot_general x6, matrix products, project(): return jnp.dot(normed, weight, preferred_element_type=jnp.float32)  5.83 us
    dot_general x1, matrix products, cell_step(): jnp.einsum('bhd,bhde->bhe', queries, new_cell, precision=lax.Precision.HI...  5.45 us
  transfers between devices with their start and end apart: 6, of which 4 were waited for; matrix products, arithmetic and copies ran while one was open for 30% of the time, Pallas kernels for 0%

commit v1 on v0

v1 whole, which is shorter than its diff:
```python
import functools

import jax
import jax.numpy as jnp
from jax import lax
from jax.experimental import pallas as pl
from jax.experimental.pallas import tpu as pltpu
from jax.sharding import PartitionSpec as P

EPS = 1e-06
MESH = pl.DeviceIdType.MESH
F32 = jnp.float32
BF16 = jnp.bfloat16
NT = (((1,), (1,)), ((), ()))


def dot(a, b):
    return jnp.dot(a, b, preferred_element_type=F32)


def dot_nt(a, b):
    return lax.dot_general(a, b, NT, preferred_element_type=F32)


CHUNK = 6
N_CHUNK = 8


def cell_kernel(
    tok_h, gain_h, wq_h, wk_h, wv_h, wo_h, win_h, wf_h, inb, fb, cell_h, norm_h, max_h,
    mixed_o, cell_o, norm_o, max_o,
    tok, gain, wts, win, wf, cell, norm, mx, normed, vs, cb, qt, wt, num,
    wsem, csem, osem, ssem,
):
    small = [
        pltpu.make_async_copy(src, dst, ssem.at[i])
        for i, (src, dst) in enumerate(
            [(tok_h, tok), (gain_h, gain), (win_h, win), (wf_h, wf), (norm_h, norm), (max_h, mx)]
        )
    ]
    for cp in small:
        cp.start()
    wcp = [pltpu.make_async_copy(src, wts.at[i], wsem.at[i]) for i, src in enumerate([wq_h, wk_h, wv_h, wo_h])]
    for cp in wcp:
        cp.start()

    def cin(i):
        s = pl.ds(i * CHUNK, CHUNK)
        return pltpu.make_async_copy(cell_h.at[s], cell.at[s], csem.at[i])

    def cout(i):
        s = pl.ds(i * CHUNK, CHUNK)
        return pltpu.make_async_copy(cell.at[s], cell_o.at[s], osem.at[i])

    for i in range(N_CHUNK):
        cin(i).start()
    for cp in small:
        cp.wait()

    xf = tok[...].astype(F32)
    ms = jnp.mean(xf * xf, axis=-1, keepdims=True)
    normed[...] = (xf * lax.rsqrt(ms + EPS) * gain[...]).astype(BF16)
    nb = normed[...]
    in_pre = dot_nt(win[...], nb)
    fpre = dot_nt(wf[...], nb)
    hrow = lax.broadcasted_iota(jnp.int32, in_pre.shape, 0)
    in_pre = in_pre + jnp.where(hrow == 0, inb[0], inb[1])
    fpre = fpre + jnp.where(hrow == 0, fb[0], fb[1])
    log_f = jnp.minimum(fpre, 0.0) - jnp.log1p(jnp.exp(-jnp.abs(fpre)))
    lm = log_f + mx[...]
    new_max = jnp.maximum(lm, in_pre)
    max_o[...] = new_max
    carry = jnp.exp(lm - new_max)
    write = jnp.exp(in_pre - new_max)
    floor = jnp.exp(-new_max)
    rows = jnp.concatenate([carry, write, floor], axis=0)
    rows = jnp.concatenate([rows, jnp.zeros((6, 80), F32)], axis=1)
    rows = jnp.concatenate([rows, jnp.zeros((122, 128), F32)], axis=0)
    cols = rows.T

    wcp[0].wait()
    q = dot(nb, wts[0])
    wcp[1].wait()
    k = dot(nb, wts[1]) * (128 ** (-0.5))
    wcp[2].wait()
    v = dot(nb, wts[2])
    vs[0] = v[:, 0:128]
    vs[1] = v[:, 128:256]
    wcp[3].wait()
    og = jax.nn.sigmoid(dot(nb, wts[3]))

    denom = []
    pad = jnp.zeros((80, 128), F32)
    for h in range(2):
        ca = jnp.broadcast_to(cols[0:48, h : h + 1], (48, 128))
        wr = jnp.broadcast_to(cols[0:48, 2 + h : 3 + h], (48, 128))
        qh = q[:, h * 128 : (h + 1) * 128]
        written = wr * k[:, h * 128 : (h + 1) * 128]
        hs = pl.ds(h, 48, stride=2)
        nn = ca * norm[hs, :] + written
        norm_o[hs, :] = nn
        den = jnp.sum(qh * nn, axis=-1, keepdims=True)
        denom.append(jnp.maximum(jnp.abs(den), cols[0:48, 4 + h : 5 + h]))
        cb[h] = ca
        qt[h] = jnp.concatenate([qh, pad], axis=0).T
        wt[h] = jnp.concatenate([written, pad], axis=0).T

    def step(i, _):
        cin(i).wait()
        shift = lax.rem(128 - i * CHUNK, 128)
        for h in range(2):
            qi = pltpu.roll(qt[h], shift, 1)
            wi = pltpu.roll(wt[h], shift, 1)
            for j in range(CHUNK):
                b = i * CHUNK + j
                row = pl.ds(b, 1)
                new = cb[h, row, :] * cell[b, h] + wi[:, j : j + 1] * vs[h, row, :]
                cell[b, h] = new
                num[h, row, :] = jnp.sum(qi[:, j : j + 1] * new, axis=0, keepdims=True)
        cout(i).start()
        return 0

    lax.fori_loop(0, N_CHUNK, step, 0)
    for h in range(2):
        lanes = slice(h * 128, (h + 1) * 128)
        mixed_o[:, lanes] = (og[:, lanes] * (num[h] / denom[h])).astype(BF16)
    for i in range(N_CHUNK):
        cout(i).wait()


def cell_call(*args):
    any_ = pl.BlockSpec(memory_space=pl.ANY)
    vm = pl.BlockSpec(memory_space=pltpu.VMEM)
    sm = pl.BlockSpec(memory_space=pltpu.SMEM)
    return pl.pallas_call(
        cell_kernel,
        out_shape=(
            jax.ShapeDtypeStruct((48, 256), BF16),
            jax.ShapeDtypeStruct((48, 2, 128, 128), F32),
            jax.ShapeDtypeStruct((96, 128), F32),
            jax.ShapeDtypeStruct((2, 48), F32),
        ),
        in_specs=[any_] * 8 + [sm, sm] + [any_] * 3,
        out_specs=(vm, any_, vm, vm),
        scratch_shapes=[
            pltpu.VMEM((48, 2048), BF16),
            pltpu.VMEM((1, 2048), F32),
            pltpu.VMEM((4, 2048, 256), BF16),
            pltpu.VMEM((2, 2048), BF16),
            pltpu.VMEM((2, 2048), BF16),
            pltpu.VMEM((48, 2, 128, 128), F32),
            pltpu.VMEM((96, 128), F32),
            pltpu.VMEM((2, 48), F32),
            pltpu.VMEM((48, 2048), BF16),
            pltpu.VMEM((2, 48, 128), F32),
            pltpu.VMEM((2, 48, 128), F32),
            pltpu.VMEM((2, 128, 128), F32),
            pltpu.VMEM((2, 128, 128), F32),
            pltpu.VMEM((2, 48, 128), F32),
            pltpu.SemaphoreType.DMA((4,)),
            pltpu.SemaphoreType.DMA((N_CHUNK,)),
            pltpu.SemaphoreType.DMA((N_CHUNK,)),
            pltpu.SemaphoreType.DMA((6,)),
        ],
        compiler_params=pltpu.CompilerParams(vmem_limit_bytes=20 * 2**20),
        name="cell",
    )(*args)


REL = [
    (0, 0), (1, 0), (3, 0), (0, 1), (0, 3),
    (1, 1), (1, 3), (3, 1), (3, 3), (2, 0), (0, 2),
    (2, 1), (2, 3), (1, 2), (3, 2),
    (2, 2),
]
IDX = {rel: i for i, rel in enumerate(REL)}
GROUPS = [(0, 5), (5, 6), (11, 4), (15, 1)]
ZP, ZM, YP, YM = (1, 0), (3, 0), (0, 1), (0, 3)
N_MSG = 160


def layer_kernel(
    mixed_h, tok_h, wmix_h, gain_h, bg_h, ids_h, rw_h, gate_h, up_h, down_h, eg_h, eu_h, ed_h,
    out,
    ah, tok, wmix, gain, bg, ids, rw, w, d, eg, eu, ed, meta, g, res, hid, xo, xp, xb, xs, eh, sb, rsr, rb, eret,
    ssem, rsem, lsem,
):
    me = lax.axis_index("ep")
    x = lax.axis_index("tp")
    c = lax.rem(me, 2)
    zy = lax.div(me, 2)
    y = lax.rem(zy, 4)
    z = lax.div(zy, 4)

    def dev(dz, dy, dx, pc):
        zz = lax.rem(z + dz, 4)
        yy = lax.rem(y + dy, 4)
        cc = 1 - c if pc else c
        return ((zz * 4 + yy) * 2 + cc, lax.rem(x + dx, 4))

    count = [0]
    sent = []

    class Msg:
        def __init__(self, src, dst, device, land=None):
            n = count[0]
            count[0] += 1
            self.copy = pltpu.make_async_remote_copy(
                src_ref=src, dst_ref=dst, send_sem=ssem.at[n], recv_sem=rsem.at[n], device_id=device, device_id_type=MESH
            )

        def start(self):
            self.copy.start()
            sent.append(self.copy)
            return self

        def arrived(self):
            self.copy.wait_recv()

    local = []

    def load(src, dst):
        cp = pltpu.make_async_copy(src, dst, lsem.at[len(local)])
        local.append(cp)
        cp.start()
        return cp

    barrier = pltpu.get_barrier_semaphore()
    peers = [dev(0, 0, 1, 0), dev(0, 0, 2, 0), dev(0, 0, 3, 0), dev(0, 0, 0, 1)]
    peers += [dev(dz, dy, 0, 0) for dz, dy in (ZP, ZM, YP, YM)]
    for peer in peers:
        pl.semaphore_signal(barrier, inc=1, device_id=peer, device_id_type=MESH)

    mine = pl.ds(pl.multiple_of(x * 256, 256), 256)
    cp_mixed = load(mixed_h, ah.at[:, mine])
    cp_ids = load(ids_h, ids)
    cp_rw = load(rw_h, rw)
    cp_tok = load(tok_h, tok)
    cp_gain = load(gain_h, gain)
    cp_bg = load(bg_h, bg)
    cp_wmix = load(wmix_h, wmix)
    cp_gate = load(gate_h, w.at[0:64])
    cp_up = load(up_h, w.at[128:192])
    cols = pl.ds(pl.multiple_of(x * 512, 512), 512)
    cp_down = load(down_h.at[:, cols], d.at[0:64])
    cp_ed = load(ed_h.at[:, cols], ed.at[0:256])
    cp_eg = load(eg_h, eg)
    cp_eu = load(eu_h, eu)

    cp_ids.wait()
    cp_rw.wait()
    idf = ids[...].astype(F32)
    four = jnp.concatenate([idf, rw[...]], axis=0)
    four = jnp.concatenate([four, jnp.zeros((4, 80), F32)], axis=1)
    four = jnp.concatenate([four, jnp.zeros((124, 128), F32)], axis=0)
    idc = four.T
    before = lax.broadcasted_iota(jnp.int32, (48, 48), 0) < lax.broadcasted_iota(jnp.int32, (48, 48), 1)
    slots = []
    for ch in range(2):
        row = idf[ch : ch + 1, :]
        hits = jnp.where(idc[0:48, 0:1] == row, 1.0, 0.0) + jnp.where(idc[0:48, 1:2] == row, 1.0, 0.0)
        rank = jnp.sum(jnp.where(before, hits, 0.0), axis=0, keepdims=True)
        slots.append(row * 16.0 + rank)
    srow = jnp.concatenate(slots + [jnp.zeros((6, 48), F32)], axis=0)
    srow = jnp.concatenate([srow, jnp.zeros((8, 80), F32)], axis=1)
    meta[zy] = srow
    scol = jnp.concatenate([srow, jnp.zeros((120, 128), F32)], axis=0).T

    pl.semaphore_wait(barrier, len(peers))

    cp_mixed.wait()
    heads = [Msg(ah.at[:, mine], ah.at[:, mine], dev(0, 0, dx, 0)).start() for dx in (1, 3, 2)]
    m_z = [Msg(meta.at[zy], meta.at[zy], dev(*k, 0, 0)).start() for k in (ZP, ZM)]
    w_p = [
        Msg(gate_h, w.at[64:128], dev(0, 0, 0, 1)).start(),
        Msg(up_h, w.at[192:256], dev(0, 0, 0, 1)).start(),
    ]
    down_x, ed_x = {}, {}
    for dx in (1, 3, 2):
        their = pl.ds(pl.multiple_of(lax.rem(x + dx, 4) * 512, 512), 512)
        s = (4 - dx) % 4
        down_x[s] = Msg(down_h.at[:, their], d.at[s * 128 : s * 128 + 64], dev(0, 0, dx, 0)).start()
        ed_x[s] = Msg(ed_h.at[:, their], ed.at[s * 256 : s * 256 + 256], dev(0, 0, dx, 0)).start()
    down_p = [Msg(down_h.at[:, cols], d.at[64:128], dev(0, 0, 0, 1)).start()]

    cp_wmix.wait()
    cp_tok.wait()
    cp_gain.wait()
    cp_bg.wait()
    for m in heads:
        m.arrived()

    sq = jnp.zeros((48, 1), F32)
    for n in range(4):
        s = slice(n * 512, (n + 1) * 512)
        r = (tok[:, s].astype(F32) + dot(ah[...], wmix[:, s])).astype(BF16)
        res[:, s] = r
        rf = r.astype(F32)
        sq = sq + jnp.sum(rf * rf, axis=-1, keepdims=True)
    inv = lax.rsqrt(sq * (1.0 / 2048.0) + EPS)
    gate_sum = jnp.zeros((48, 1), F32)
    for n in range(4):
        s = slice(n * 512, (n + 1) * 512)
        mi = (res[:, s].astype(F32) * inv * gain[:, s]).astype(BF16)
        g[0, n] = mi
        gate_sum = gate_sum + jnp.sum(mi.astype(F32) * bg[:, s].astype(F32), axis=-1, keepdims=True)
    bw = jax.nn.sigmoid(gate_sum)

    def spread(rel, q0, nq, way):
        to = ((rel[0] - way[0]) % 4, (rel[1] - way[1]) % 4)
        q = pl.ds(q0, nq)
        return Msg(g.at[IDX[rel], q], g.at[IDX[to], q], dev(*way, 0, 0)).start()

    O = (0, 0)
    a_zp, a_zm = spread(O, 0, 2, ZP), spread(O, 0, 2, ZM)
    b_yp, b_ym = spread(O, 2, 2, YP), spread(O, 2, 2, YM)
    a_yp, a_ym = spread(O, 0, 2, YP), spread(O, 0, 2, YM)
    b_zp, b_zm = spread(O, 2, 2, ZP), spread(O, 2, 2, ZM)

    for m in m_z:
        m.arrived()
    zmy = lax.rem(z + 3, 4) * 4 + y
    m_z2 = Msg(meta.at[zmy], meta.at[zmy], dev(*ZP, 0, 0)).start()

    a_zp.arrived()
    f_z0 = spread((3, 0), 0, 1, ZP)
    t_33, t_31 = spread((3, 0), 0, 2, YP), spread((3, 0), 0, 2, YM)
    a_zm.arrived()
    f_z1 = spread((1, 0), 1, 1, ZM)
    t_13, t_11 = spread((1, 0), 0, 2, YP), spread((1, 0), 0, 2, YM)
    b_yp.arrived()
    f_y2 = spread((0, 3), 2, 1, YP)
    u_33, u_13 = spread((0, 3), 2, 2, ZP), spread((0, 3), 2, 2, ZM)
    b_ym.arrived()
    f_y3 = spread((0, 1), 3, 1, YM)
    u_31, u_11 = spread((0, 1), 2, 2, ZP), spread((0, 1), 2, 2, ZM)
    a_yp.arrived()
    f_y0 = spread((0, 3), 0, 1, YP)
    a_ym.arrived()
    f_y1 = spread((0, 1), 1, 1, YM)
    b_zp.arrived()
    f_z2 = spread((3, 0), 2, 1, ZP)
    b_zm.arrived()
    f_z3 = spread((1, 0), 3, 1, ZM)

    m_z2.arrived()
    m_y = []
    for k in (YP, YM):
        for zz in range(4):
            m_y.append(Msg(meta.at[zz * 4 + y], meta.at[zz * 4 + y], dev(*k, 0, 0)).start())

    cp_gate.wait()
    cp_up.wait()
    for m in w_p:
        m.arrived()
    cp_down.wait()
    for s in (1, 2, 3):
        down_x[s].arrived()
        own = slice(s * 128, s * 128 + 64)
        down_p.append(Msg(d.at[own], d.at[s * 128 + 64 : s * 128 + 128], dev(0, 0, 0, 1)).start())

    def up_group(n):
        r0, nb = GROUPS[n]
        acc = None
        for q in range(4):
            part = dot_nt(g[r0 : r0 + nb, q].reshape(nb * 48, 512), w[:, q * 512 : (q + 1) * 512])
            acc = part if acc is None else acc + part
        ga, up = acc[:, 0:128], acc[:, 128:256]
        rows = pl.ds(r0 * 48, nb * 48)
        hid[rows, 0:128] = (ga * jax.nn.sigmoid(ga) * up).astype(BF16)
        out = {}
        for dx in (1, 3, 2):
            s = (4 - dx) % 4
            out[s] = Msg(hid.at[rows, 0:128], hid.at[rows, s * 128 : s * 128 + 128], dev(0, 0, dx, 0)).start()
        return out

    e_mine = (me * 16).astype(F32)
    e_other = ((zy * 2 + (1 - c)) * 16).astype(F32)

    def pick_group(n):
        r0, nb = GROUPS[n]
        lane8 = lax.broadcasted_iota(jnp.int32, (8, 48), 0).astype(F32)
        code = jnp.concatenate([lane8 + e_mine, lane8 + e_other], axis=0)
        for r in range(r0, r0 + nb):
            dz, dy = REL[r]
            owner = lax.rem(z + dz, 4) * 4 + lax.rem(y + dy, 4)
            m = meta[owner]
            hit = jnp.where(m[0:1, 0:48] == code, 1.0, 0.0) + jnp.where(m[1:2, 0:48] == code, 1.0, 0.0)
            hit = hit.astype(BF16)
            for q in range(4):
                picked = dot(hit, g[r, q])
                s = slice(q * 512, (q + 1) * 512)
                xo[r * 8 : r * 8 + 8, s] = picked[0:8]
                xp[r * 8 : r * 8 + 8, s] = picked[8:16]

    def pass_rows(a, b):
        rows = slice(a, b)
        xs[rows] = xp[rows].astype(BF16)
        return Msg(xs.at[rows], xb.at[rows], dev(0, 0, 0, 1)).start()

    f_z0.arrived()
    f_z1.arrived()
    t_23, t_21 = spread((2, 0), 0, 2, YP), spread((2, 0), 0, 2, YM)
    f_y2.arrived()
    f_y3.arrived()
    u_32, u_12 = spread((0, 2), 2, 2, ZP), spread((0, 2), 2, 2, ZM)
    t_33.arrived()
    h_32a = spread((3, 3), 0, 1, YP)
    t_31.arrived()
    h_32b = spread((3, 1), 1, 1, YM)
    t_13.arrived()
    h_12a = spread((1, 3), 0, 1, YP)
    t_11.arrived()
    h_12b = spread((1, 1), 1, 1, YM)
    u_33.arrived()
    h_23a = spread((3, 3), 2, 1, ZP)
    u_13.arrived()
    h_23b = spread((1, 3), 3, 1, ZM)
    u_31.arrived()
    h_21a = spread((3, 1), 2, 1, ZP)
    u_11.arrived()
    h_21b = spread((1, 1), 3, 1, ZM)

    for m in m_y:
        m.arrived()
    m_y2 = []
    ym = lax.rem(y + 3, 4)
    for zz in range(4):
        m_y2.append(Msg(meta.at[zz * 4 + ym], meta.at[zz * 4 + ym], dev(*YP, 0, 0)).start())

    hid_in = {}
    hid_in[0] = up_group(0)
    pick_group(0)
    for m in (f_y0, f_y1, f_z2, f_z3):
        m.arrived()
    for m in m_y2:
        m.arrived()

    t_23.arrived()
    l_22a = spread((2, 3), 0, 1, YP)
    t_21.arrived()
    l_22b = spread((2, 1), 1, 1, YM)
    u_32.arrived()
    l_22c = spread((3, 2), 2, 1, ZP)
    u_12.arrived()
    l_22d = spread((1, 2), 3, 1, ZM)

    hid_in[1] = up_group(1)
    pick_group(1)

    for m in down_p:
        m.arrived()

    reduced = []

    def down_group(n):
        r0, nb = GROUPS[n]
        for m in hid_in[n].values():
            m.arrived()
        part = dot(hid[r0 * 48 : (r0 + nb) * 48, :], d[...])
        for i in range(nb):
            r = r0 + i
            blk = part[i * 48 : (i + 1) * 48].astype(BF16)
            if r == 0:
                rsr[0] = blk
            else:
                dz, dy = REL[r]
                sb[r] = blk
                back = IDX[((-dz) % 4, (-dy) % 4)]
                reduced.append(Msg(sb.at[r], rsr.at[back], dev(dz, dy, 0, 0)).start())

    for m in (h_32a, h_32b, h_12a, h_12b, h_23a, h_23b, h_21a, h_21b):
        m.arrived()
    hid_in[2] = up_group(2)
    pick_group(2)
    passed = [pass_rows(0, 112)]
    down_group(0)
    for m in (l_22a, l_22b, l_22c, l_22d):
        m.arrived()
    hid_in[3] = up_group(3)
    pick_group(3)
    passed.append(pass_rows(112, 128))

    cp_eg.wait()
    cp_eu.wait()

    def expert_up(half, rows_in):
        ga = dot(rows_in, eg[...])
        up = dot(rows_in, eu[...])
        eh[half, :, 0:256] = (ga * jax.nn.sigmoid(ga) * up).astype(BF16)
        out = []
        for dx in (1, 3, 2):
            s = (4 - dx) % 4
            out.append(Msg(eh.at[half, :, 0:256], eh.at[half, :, s * 256 : s * 256 + 256], dev(0, 0, dx, 0)).start())
        return out

    eh_in = [expert_up(0, xo[...].astype(BF16))]
    for m in passed:
        m.arrived()
    eh_in.append(expert_up(1, xb[...]))

    down_group(1)
    down_group(2)
    down_group(3)

    cp_ed.wait()
    for m in ed_x.values():
        m.arrived()
    returned = []
    for half in range(2):
        for m in eh_in[half]:
            m.arrived()
        eo = dot(eh[half], ed[...])
        for r in range(16):
            rows = slice(r * 8, r * 8 + 8)
            blk = jnp.concatenate([eo[rows, 0:256], eo[rows, 256:512]], axis=0).astype(BF16)
            if r == 0 and half == 0:
                eret[me] = blk
            else:
                dz, dy = REL[r]
                rb[half, r] = blk
                returned.append(Msg(rb.at[half, r], eret.at[me], dev(dz, dy, 0, half)).start())

    total = rsr[0].astype(F32)
    for m in reduced:
        m.arrived()
    for r in range(1, 16):
        total = total + rsr[r].astype(F32)
    own_res = res[:, cols].astype(F32)
    for m in returned:
        m.arrived()
    back = eret[...].reshape(512, 256)
    lane = lax.broadcasted_iota(jnp.int32, (48, 512), 1).astype(F32)
    for hf in range(2):
        s = slice(hf * 256, hf * 256 + 256)
        moe = jnp.zeros((48, 256), F32)
        for ch in range(2):
            want = scol[0:48, ch : ch + 1] + float(hf * 8)
            sel = jnp.where(lane == want, 1.0, 0.0).astype(BF16)
            moe = moe + dot(sel, back) * idc[0:48, 2 + ch : 3 + ch]
        out[:, s] = (own_res[:, s] + moe + bw * total[:, s]).astype(BF16)

    for cp in sent:
        cp.wait_send()


def layer_call(*args):
    any_ = pl.BlockSpec(memory_space=pl.ANY)
    vm = pl.BlockSpec(memory_space=pltpu.VMEM)
    return pl.pallas_call(
        layer_kernel,
        out_shape=jax.ShapeDtypeStruct((48, 512), BF16),
        in_specs=[any_] * 13,
        out_specs=vm,
        scratch_shapes=[
            pltpu.VMEM((48, 1024), BF16),
            pltpu.VMEM((48, 2048), BF16),
            pltpu.VMEM((1024, 2048), BF16),
            pltpu.VMEM((1, 2048), F32),
            pltpu.VMEM((1, 2048), BF16),
            pltpu.VMEM((2, 48), jnp.int32),
            pltpu.VMEM((2, 48), F32),
            pltpu.VMEM((256, 2048), BF16),
            pltpu.VMEM((512, 512), BF16),
            pltpu.VMEM((2048, 256), BF16),
            pltpu.VMEM((2048, 256), BF16),
            pltpu.VMEM((1024, 512), BF16),
            pltpu.VMEM((16, 8, 128), F32),
            pltpu.VMEM((16, 4, 48, 512), BF16),
            pltpu.VMEM((48, 2048), BF16),
            pltpu.VMEM((768, 512), BF16),
            pltpu.VMEM((128, 2048), F32),
            pltpu.VMEM((128, 2048), F32),
            pltpu.VMEM((128, 2048), BF16),
            pltpu.VMEM((128, 2048), BF16),
            pltpu.VMEM((2, 128, 1024), BF16),
            pltpu.VMEM((16, 48, 512), BF16),
            pltpu.VMEM((16, 48, 512), BF16),
            pltpu.VMEM((2, 16, 16, 256), BF16),
            pltpu.VMEM((32, 16, 256), BF16),
            pltpu.SemaphoreType.DMA((N_MSG,)),
            pltpu.SemaphoreType.DMA((N_MSG,)),
            pltpu.SemaphoreType.DMA((16,)),
        ],
        compiler_params=pltpu.CompilerParams(vmem_limit_bytes=36 * 2**20, collective_id=0, has_side_effects=True),
        name="layer",
    )(*args)


def local(
    tokens, mix_gain, w_query, w_key, w_value, w_outgate, w_ingate, w_forget, in_bias, forget_bias, w_mix_out,
    cell_state, norm_state, max_state, moe_gain, route_ids, route_weights, expert_gate, expert_up, expert_down,
    branch_gate, dense_gate, dense_up, dense_down,
):
    mixed, new_cell, new_norm, new_max = cell_call(
        tokens, mix_gain.reshape(1, 2048), w_query, w_key, w_value, w_outgate, w_ingate.T, w_forget.T,
        in_bias, forget_bias, cell_state, norm_state.reshape(96, 128), max_state.T,
    )
    layer_out = layer_call(
        mixed, tokens, w_mix_out, moe_gain.reshape(1, 2048), branch_gate.reshape(1, 2048), route_ids.T, route_weights.T,
        dense_gate.T, dense_up.T, dense_down,
        expert_gate.reshape(2048, 256), expert_up.reshape(2048, 256), expert_down.reshape(256, 2048),
    )
    return (layer_out, new_cell, new_norm.reshape(48, 2, 128), new_max.T)


def solution(mesh):
    in_specs = (
        P("ep", None),
        P(),
        P(None, "tp"),
        P(None, "tp"),
        P(None, "tp"),
        P(None, "tp"),
        P(None, "tp"),
        P(None, "tp"),
        P("tp"),
        P("tp"),
        P(),
        P("ep", "tp", None, None),
        P("ep", "tp", None),
        P("ep", "tp"),
        P(),
        P("ep", None),
        P("ep", None),
        P("ep", None, "tp"),
        P("ep", None, "tp"),
        P("ep", "tp", None),
        P(),
        P(None, ("ep", "tp")),
        P(None, ("ep", "tp")),
        P(("ep", "tp"), None),
    )
    out_specs = (P("ep", "tp"), P("ep", "tp", None, None), P("ep", "tp", None), P("ep", "tp"))
    return jax.shard_map(local, mesh=mesh, in_specs=in_specs, out_specs=out_specs, check_vma=False)
```

time: 161 us -> 82.8 us (0.51)
  Pallas kernels: 0 us -> 66.5 us
  blocking collectives: 40.4 us -> 0 us
  waiting for transfers between devices: 35 us -> 0 us
  matrix products: 30.7 us -> 0 us
  starting transfers between devices: 17.9 us -> 0 us
  between operations: 14.6 us -> 0.81 us
  other arithmetic: 12.2 us -> 0 us
  local copies, waits for them, and re-layouts: 8.5 us -> 14.9 us
    pallas_call x0 -> x2, Pallas kernels: none -> 66.5 us  [the longest x1 54.4 us: layer_call(): pl.pallas_call(layer_kernel, out_shape=jax.ShapeDtypeStruct((48, 512), BF...]
    all_to_all x2 -> x0, blocking collectives: 40.4 us -> none  [the longest x1 29.8 us: local(): lax.all_to_all(dispatch, 'ep', split_axis=0, concat_axis=0, tiled=True)]
    all_to_all x4 -> x0, waiting for transfers between devices: 32.9 us -> none  [the longest x2 31.6 us: summed_on_arrival(): lax.all_to_all(parts, axis, split_axis=0, concat_axis=0, tiled=True)]
    dot_general x13 -> x0, matrix products: 30.7 us -> none  [the longest x1 7.52 us: local(): jnp.dot(hidden, down_block, preferred_element_type=jnp.float32)]
    all_to_all x4 -> x0, starting transfers between devices: 17.8 us -> none  [the longest x2 9.53 us: summed_on_arrival(): lax.all_to_all(parts, axis, split_axis=0, concat_axis=0, tiled=True)]
    unnamed x35 -> x49, local copies, waits for them, and re-layouts: 0.28 us -> 14.2 us
    add x2 -> x0, other arithmetic: 4.67 us -> none  [the longest x1 4.67 us: cell_step(): carry_factor[..., None, None] * cell_state]
    reduce_sum x7 -> x0, other arithmetic: 3.69 us -> none  [the longest x1 1.62 us: cell_step(): denominator = jnp.sum(queries * new_norm, axis=-1)]
  transfers between devices with their start and end apart: 6 -> 0, of which waited for: 4 -> 0; matrix products, arithmetic and copies ran while one was open for 30% -> 0% of each run, Pallas kernels for 0% -> 0%
where the time goes in v1:
time: 82.8 us; the launch traced here: 82.2 us
  Pallas kernels  66.5 us (80%)
  local copies, waits for them, and re-layouts  14.9 us (18%)
    pallas_call x1, Pallas kernels, layer_call(): pl.pallas_call(layer_kernel, out_shape=jax.ShapeDtypeStruct((48, 512), BF...  54.4 us
    unnamed x49, local copies, waits for them, and re-layouts  14.2 us
    pallas_call x1, Pallas kernels, cell_call(): pl.pallas_call(cell_kernel, out_shape=(jax.ShapeDtypeStruct((48, 256), BF...  12.1 us

profile of v1, /device:TPU:1, one launch (start us, length us, event | category | flops | bytes accessed | tf_op | source)
XLA Modules:
  0.0 82.2 jit_solution(5944584886337694355)
XLA Ops:
  0.6 0.0 copy-start.21
  0.6 0.0 copy-start.20
  0.7 0.0 copy-start.18
  0.7 0.7 reshape.35.bg_h
  1.4 2.8 %copy-done = f32[48,2,128,128]{3,2,1,0:T(8,128)S(1)} copy-done((f32[48,2,128,128]{3,2,1,0:T(8,128)S(1)}, f32[48,2,128,128]{3,2,1,0:T(8,128)}, u32[]{:S(2)}) %copy-start) | copy-done | bytes 6291480
  4.2 1.2 %copy-done.2 = bf16[2048,256]{1,0:T(8,128)(2,1)S(1)} copy-done((bf16[2048,256]{1,0:T(8,128)(2,1)S(1)}, bf16[2048,256]{1,0:T(8,128)(2,1)}, u32[]{:S(2)}) %copy-start.2) | copy-done | bytes 1048600
  5.4 1.2 %copy-done.3 = bf16[2048,256]{1,0:T(8,128)(2,1)S(1)} copy-done((bf16[2048,256]{1,0:T(8,128)(2,1)S(1)}, bf16[2048,256]{1,0:T(8,128)(2,1)}, u32[]{:S(2)}) %copy-start.3) | copy-done | bytes 1048600
  6.6 1.2 %copy-done.4 = bf16[2048,256]{1,0:T(8,128)(2,1)S(1)} copy-done((bf16[2048,256]{1,0:T(8,128)(2,1)S(1)}, bf16[2048,256]{1,0:T(8,128)(2,1)}, u32[]{:S(2)}) %copy-start.4) | copy-done | bytes 1048600
  7.8 1.2 %copy-done.5 = bf16[2048,256]{1,0:T(8,128)(2,1)S(1)} copy-done((bf16[2048,256]{1,0:T(8,128)(2,1)S(1)}, bf16[2048,256]{1,0:T(8,128)(2,1)}, u32[]{:S(2)}) %copy-start.5) | copy-done | bytes 1048600
  9.1 0.9 %copy-done.9 = bf16[48,2048]{1,0:T(8,128)(2,1)S(1)} copy-done((bf16[48,2048]{1,0:T(8,128)(2,1)S(1)}, bf16[48,2048]{1,0:T(8,128)(2,1)}, u32[]{:S(2)}) %copy-start.9) | copy-done | bytes 196632
  10.0 0.8 copy-done.14
  10.8 0.7 copy-done.15
  11.5 0.7 copy-done.16
  12.2 0.7 copy-done.17
  12.9 0.7 copy-done.19
  13.6 0.7 copy-done.22
  14.2 0.7 copy-done.23
  14.9 0.0 copy-start.11
  14.9 0.0 copy-start.12
  14.9 0.0 copy-start.13
  14.9 12.1 %cell.1 = (bf16[48,256]{1,0:T(8,128)(2,1)S(1)}, f32[48,2,128,128]{3,2,1,0:T(8,128)}, f32[96,128]{1,0:T(8,128)}, f32[2,48]{1,0:T(2,128)}) custom-call(bf16[48,2048]{1,0:T(8,128)(2,1)S(1)} %copy-done.9, f32[1,2048]{1,0:T(1,128)S(1)} %bitcast.21, bf16[2048,256]{1,0:T(8,128)(2,1)S(1)} %copy-done.2, bf16[2048,256]{1,0:T(8,128)(2,1)S(1)} %copy-done.3, ...), custom_call_target="tpu_custom_call" | custom-call | tf_op jit(solution)/shard_map/cell/pallas_call | solution.py:135
  27.0 0.0 copy-done.21
  27.0 0.0 copy-done.20
  27.1 0.0 copy-done.18
  27.1 0.0 copy-done.1
  27.1 0.0 copy-done.6
  27.1 0.0 copy-done.7
  27.1 0.0 copy-done.8
  27.1 0.0 copy-done.10
  27.1 0.0 copy-done.11
  27.1 54.4 %layer.1 = bf16[48,512]{1,0:T(8,128)(2,1)S(1)} custom-call(bf16[48,256]{1,0:T(8,128)(2,1)S(1)} %get-tuple-element.8.mixed_h, bf16[48,2048]{1,0:T(8,128)(2,1)S(1)} %copy-done.10, bf16[1024,2048]{1,0:T(8,128)(2,1)S(1)} %copy-done.1, f32[1,2048]{1,0:T(1,128)S(1)} %bitcast.24, bf16[1,2048]{1,0:T(2,128)(2,1)S(1)} %reshape.35.bg_h, s32[2,48]{1,0:T(2,128)S(1)} %bitcast.26, ...), custom_call_target="tpu_custom_call" | custom-call | tf_op jit(solution)/shard_map/layer/pallas_call | solution.py:550
  81.6 0.6 copy.29
  (20 shorter events, 0.0 us)
Async XLA Ops:
  0.6 26.4 %copy-start.21 = (f32[48,2]{0,1:T(2,128)S(1)}, f32[48,2]{0,1:T(2,128)}, u32[]{:S(2)}) copy-start(f32[48,2]{0,1:T(2,128)} %param.40) | copy-start | bytes 1156
  0.6 26.4 %copy-start.20 = (s32[48,2]{0,1:T(2,128)S(1)}, s32[48,2]{0,1:T(2,128)}, u32[]{:S(2)}) copy-start(s32[48,2]{0,1:T(2,128)} %param.39) | copy-start | bytes 1156
  0.7 26.4 %copy-start.18 = (f32[2048]{0:T(1024)S(1)}, f32[2048]{0:T(1024)}, u32[]{:S(2)}) copy-start(f32[2048]{0:T(1024)} %param.38) | copy-start | bytes 24580
  1.4 2.8 %copy-start = (f32[48,2,128,128]{3,2,1,0:T(8,128)S(1)}, f32[48,2,128,128]{3,2,1,0:T(8,128)}, u32[]{:S(2)}) copy-start(f32[48,2,128,128]{3,2,1,0:T(8,128)} %cell_h.1) | copy-start | bytes 18874372
  4.2 1.2 %copy-start.2 = (bf16[2048,256]{1,0:T(8,128)(2,1)S(1)}, bf16[2048,256]{1,0:T(8,128)(2,1)}, u32[]{:S(2)}) copy-start(bf16[2048,256]{1,0:T(8,128)(2,1)} %wq_h.1) | copy-start | bytes 3145732
  5.4 1.2 %copy-start.3 = (bf16[2048,256]{1,0:T(8,128)(2,1)S(1)}, bf16[2048,256]{1,0:T(8,128)(2,1)}, u32[]{:S(2)}) copy-start(bf16[2048,256]{1,0:T(8,128)(2,1)} %wk_h.1) | copy-start | bytes 3145732
  6.6 1.2 %copy-start.4 = (bf16[2048,256]{1,0:T(8,128)(2,1)S(1)}, bf16[2048,256]{1,0:T(8,128)(2,1)}, u32[]{:S(2)}) copy-start(bf16[2048,256]{1,0:T(8,128)(2,1)} %wv_h.1) | copy-start | bytes 3145732
  7.8 1.2 %copy-start.5 = (bf16[2048,256]{1,0:T(8,128)(2,1)S(1)}, bf16[2048,256]{1,0:T(8,128)(2,1)}, u32[]{:S(2)}) copy-start(bf16[2048,256]{1,0:T(8,128)(2,1)} %wo_h.1) | copy-start | bytes 3145732
  9.1 0.9 %copy-start.9 = (bf16[48,2048]{1,0:T(8,128)(2,1)S(1)}, bf16[48,2048]{1,0:T(8,128)(2,1)}, u32[]{:S(2)}) copy-start(bf16[48,2048]{1,0:T(8,128)(2,1)} %tok_h.3) | copy-start | bytes 589828
  10.0 0.8 copy-start.14
  10.8 0.7 copy-start.15
  11.5 0.7 copy-start.16
  12.2 0.7 copy-start.17
  12.9 0.7 copy-start.19
  13.6 0.7 copy-start.22
  14.2 0.7 copy-start.23
  14.9 12.2 %copy-start.1 = (bf16[1024,2048]{1,0:T(8,128)(2,1)S(1)}, bf16[1024,2048]{1,0:T(8,128)(2,1)}, u32[]{:S(2)}) copy-start(bf16[1024,2048]{1,0:T(8,128)(2,1)} %wmix_h.1) | copy-start | bytes 12582916
  14.9 12.2 %copy-start.6 = (bf16[1,2048,256]{2,1,0:T(8,128)(2,1)S(1)}, bf16[1,2048,256]{2,1,0:T(8,128)(2,1)}, u32[]{:S(2)}) copy-start(bf16[1,2048,256]{2,1,0:T(8,128)(2,1)} %param.41) | copy-start | bytes 3145732
  14.9 12.2 %copy-start.7 = (bf16[1,2048,256]{2,1,0:T(8,128)(2,1)S(1)}, bf16[1,2048,256]{2,1,0:T(8,128)(2,1)}, u32[]{:S(2)}) copy-start(bf16[1,2048,256]{2,1,0:T(8,128)(2,1)} %param.42) | copy-start | bytes 3145732
  14.9 12.2 %copy-start.8 = (bf16[1,256,2048]{2,1,0:T(8,128)(2,1)S(1)}, bf16[1,256,2048]{2,1,0:T(8,128)(2,1)}, u32[]{:S(2)}) copy-start(bf16[1,256,2048]{2,1,0:T(8,128)(2,1)} %param.43) | copy-start | bytes 3145732
  14.9 12.2 %copy-start.10 = (bf16[48,2048]{1,0:T(8,128)(2,1)S(1)}, bf16[48,2048]{1,0:T(8,128)(2,1)}, u32[]{:S(2)}) copy-start(bf16[48,2048]{1,0:T(8,128)(2,1)} %tok_h.3) | copy-start | bytes 589828
  14.9 12.2 %copy-start.11 = (bf16[2048,64]{0,1:T(8,128)(2,1)S(1)}, bf16[2048,64]{0,1:T(8,128)(2,1)}, u32[]{:S(2)}) copy-start(bf16[2048,64]{0,1:T(8,128)(2,1)} %param.45) | copy-start | bytes 786436
  14.9 12.2 %copy-start.12 = (bf16[2048,64]{0,1:T(8,128)(2,1)S(1)}, bf16[2048,64]{0,1:T(8,128)(2,1)}, u32[]{:S(2)}) copy-start(bf16[2048,64]{0,1:T(8,128)(2,1)} %param.46) | copy-start | bytes 786436
  14.9 12.2 %copy-start.13 = (bf16[64,2048]{1,0:T(8,128)(2,1)S(1)}, bf16[64,2048]{1,0:T(8,128)(2,1)}, u32[]{:S(2)}) copy-start(bf16[64,2048]{1,0:T(8,128)(2,1)} %down_h.1) | copy-start | bytes 786436

commit v2 on v1

v2 whole, which is shorter than its diff:
```python
import functools

import jax
import jax.numpy as jnp
from jax import lax
from jax.experimental import pallas as pl
from jax.experimental.pallas import tpu as pltpu
from jax.sharding import PartitionSpec as P

EPS = 1e-06
MESH = pl.DeviceIdType.MESH
F32 = jnp.float32
BF16 = jnp.bfloat16
NT = (((1,), (1,)), ((), ()))


def dot(a, b):
    return jnp.dot(a, b, preferred_element_type=F32)


def dot_nt(a, b):
    return lax.dot_general(a, b, NT, preferred_element_type=F32)


CHUNK = 6
N_CHUNK = 8


def split3(a):
    first = a.astype(BF16).astype(F32)
    rest = a - first
    second = rest.astype(BF16).astype(F32)
    return first, second, rest - second


def as_columns(rows):
    n, width = rows.shape
    wide = jnp.concatenate([rows, jnp.zeros((n, 128 - width), F32)], axis=1) if width < 128 else rows
    return jnp.concatenate([wide, jnp.zeros((128 - n, 128), F32)], axis=0).T


def slot_rows(ids):
    idf = ids.astype(F32)
    idc = as_columns(idf)
    before = lax.broadcasted_iota(jnp.int32, (48, 48), 0) < lax.broadcasted_iota(jnp.int32, (48, 48), 1)
    slots = []
    for ch in range(2):
        row = idf[ch : ch + 1, :]
        hits = jnp.where(idc[0:48, 0:1] == row, 1.0, 0.0) + jnp.where(idc[0:48, 1:2] == row, 1.0, 0.0)
        rank = jnp.sum(jnp.where(before, hits, 0.0), axis=0, keepdims=True)
        slots.append(row * 16.0 + rank)
    srow = jnp.concatenate(slots + [jnp.zeros((6, 48), F32)], axis=0)
    return jnp.concatenate([srow, jnp.zeros((8, 80), F32)], axis=1)


def cell_kernel(
    tok_h, gain_h, wq_h, wk_h, wv_h, wo_h, win_h, wf_h, inb, fb, cell_h, norm_h, max_h, ids_h,
    mixed_o, cell_o, norm_o, max_o, slot_o,
    tok, gain, wts, win, wf, cell, norm, mx, ids, normed, vs, cb, qt, wt, num,
    wsem, csem, osem, ssem,
):
    small = [
        pltpu.make_async_copy(src, dst, ssem.at[i])
        for i, (src, dst) in enumerate(
            [(tok_h, tok), (gain_h, gain), (win_h, win), (wf_h, wf), (norm_h, norm), (max_h, mx), (ids_h, ids)]
        )
    ]
    for cp in small:
        cp.start()
    wcp = [pltpu.make_async_copy(src, wts.at[i], wsem.at[i]) for i, src in enumerate([wq_h, wk_h, wv_h, wo_h])]
    for cp in wcp:
        cp.start()

    def cin(i):
        s = pl.ds(i * CHUNK, CHUNK)
        return pltpu.make_async_copy(cell_h.at[s], cell.at[s], csem.at[i])

    def cout(i):
        s = pl.ds(i * CHUNK, CHUNK)
        return pltpu.make_async_copy(cell.at[s], cell_o.at[s], osem.at[i])

    for cp in small:
        cp.wait()
    slot_o[...] = slot_rows(ids[...])

    xf = tok[...].astype(F32)
    ms = jnp.mean(xf * xf, axis=-1, keepdims=True)
    normed[...] = (xf * lax.rsqrt(ms + EPS) * gain[...]).astype(BF16)
    nb = normed[...]
    in_pre = dot_nt(win[...], nb)
    fpre = dot_nt(wf[...], nb)
    hrow = lax.broadcasted_iota(jnp.int32, in_pre.shape, 0)
    in_pre = in_pre + jnp.where(hrow == 0, inb[0], inb[1])
    fpre = fpre + jnp.where(hrow == 0, fb[0], fb[1])
    log_f = jnp.minimum(fpre, 0.0) - jnp.log1p(jnp.exp(-jnp.abs(fpre)))
    lm = log_f + mx[...]
    new_max = jnp.maximum(lm, in_pre)
    max_o[...] = new_max
    carry = jnp.exp(lm - new_max)
    write = jnp.exp(in_pre - new_max)
    floor = jnp.exp(-new_max)
    rows = jnp.concatenate([carry, write, floor], axis=0)
    rows = jnp.concatenate([rows, jnp.zeros((6, 80), F32)], axis=1)
    rows = jnp.concatenate([rows, jnp.zeros((122, 128), F32)], axis=0)
    cols = rows.T

    wcp[0].wait()
    for i in range(2):
        cin(i).start()
    q = dot(nb, wts[0])
    wcp[1].wait()
    for i in range(2, 5):
        cin(i).start()
    k = dot(nb, wts[1]) * (128 ** (-0.5))
    wcp[2].wait()
    for i in range(5, N_CHUNK):
        cin(i).start()
    v = dot(nb, wts[2])
    for h in range(2):
        v1, v2, _ = split3(v[:, h * 128 : (h + 1) * 128])
        vs[h] = jnp.concatenate([v1, v1, v2], axis=0).astype(BF16)
    wcp[3].wait()
    og = jax.nn.sigmoid(dot(nb, wts[3]))

    denom = []
    pad = jnp.zeros((112, 128), F32)
    for h in range(2):
        ca = jnp.broadcast_to(cols[0:48, h : h + 1], (48, 128))
        wr = jnp.broadcast_to(cols[0:48, 2 + h : 3 + h], (48, 128))
        qh = q[:, h * 128 : (h + 1) * 128]
        written = wr * k[:, h * 128 : (h + 1) * 128]
        hs = pl.ds(h, 48, stride=2)
        nn = ca * norm[hs, :] + written
        norm_o[hs, :] = nn
        den = jnp.sum(qh * nn, axis=-1, keepdims=True)
        denom.append(jnp.maximum(jnp.abs(den), cols[0:48, 4 + h : 5 + h]))
        cb[h] = ca
        q1, q2, q3 = split3(qh)
        qt[h] = jnp.concatenate([q1, q2, q3, pad], axis=0).T[:, 0:144].astype(BF16)
        w1, w2, _ = split3(written)
        wt[h] = jnp.concatenate([w1, w2, w1, pad], axis=0).T[:, 0:144].astype(BF16)

    token = lax.rem(lax.broadcasted_iota(jnp.int32, (144, 128), 0), 48)

    def step(i, _):
        cin(i).wait()
        here = [token == i * CHUNK + j for j in range(CHUNK)]
        ones = jnp.concatenate([jnp.where(m, 1.0, 0.0) for m in here], axis=1).astype(BF16)
        for h in range(2):
            vh = vs[h].astype(F32)
            vrows = jnp.concatenate([jnp.where(m, vh, 0.0) for m in here], axis=1).astype(BF16)
            outer = dot(wt[h], vrows)
            qcols = dot(qt[h], ones)
            for j in range(CHUNK):
                b = i * CHUNK + j
                row = pl.ds(b, 1)
                lanes = slice(j * 128, (j + 1) * 128)
                new = cb[h, row, :] * cell[b, h] + outer[:, lanes]
                cell[b, h] = new
                num[h, row, :] = jnp.sum(qcols[:, lanes] * new, axis=0, keepdims=True)
        cout(i).start()
        return 0

    lax.fori_loop(0, N_CHUNK, step, 0)
    for h in range(2):
        lanes = slice(h * 128, (h + 1) * 128)
        mixed_o[:, lanes] = (og[:, lanes] * (num[h] / denom[h])).astype(BF16)
    for i in range(N_CHUNK):
        cout(i).wait()


def cell_call(*args):
    any_ = pl.BlockSpec(memory_space=pl.ANY)
    vm = pl.BlockSpec(memory_space=pltpu.VMEM)
    sm = pl.BlockSpec(memory_space=pltpu.SMEM)
    return pl.pallas_call(
        cell_kernel,
        out_shape=(
            jax.ShapeDtypeStruct((48, 256), BF16),
            jax.ShapeDtypeStruct((48, 2, 128, 128), F32),
            jax.ShapeDtypeStruct((96, 128), F32),
            jax.ShapeDtypeStruct((2, 48), F32),
            jax.ShapeDtypeStruct((8, 128), F32),
        ),
        in_specs=[any_] * 8 + [sm, sm] + [any_] * 4,
        out_specs=(vm, any_, vm, vm, vm),
        scratch_shapes=[
            pltpu.VMEM((48, 2048), BF16),
            pltpu.VMEM((1, 2048), F32),
            pltpu.VMEM((4, 2048, 256), BF16),
            pltpu.VMEM((2, 2048), BF16),
            pltpu.VMEM((2, 2048), BF16),
            pltpu.VMEM((48, 2, 128, 128), F32),
            pltpu.VMEM((96, 128), F32),
            pltpu.VMEM((2, 48), F32),
            pltpu.VMEM((2, 48), jnp.int32),
            pltpu.VMEM((48, 2048), BF16),
            pltpu.VMEM((2, 144, 128), BF16),
            pltpu.VMEM((2, 48, 128), F32),
            pltpu.VMEM((2, 128, 144), BF16),
            pltpu.VMEM((2, 128, 144), BF16),
            pltpu.VMEM((2, 48, 128), F32),
            pltpu.SemaphoreType.DMA((4,)),
            pltpu.SemaphoreType.DMA((N_CHUNK,)),
            pltpu.SemaphoreType.DMA((N_CHUNK,)),
            pltpu.SemaphoreType.DMA((7,)),
        ],
        compiler_params=pltpu.CompilerParams(vmem_limit_bytes=67043328),
        name="cell",
    )(*args)


REL = [
    (0, 0), (1, 0), (3, 0), (0, 1), (0, 3),
    (1, 1), (1, 3), (3, 1), (3, 3), (2, 0), (0, 2),
    (2, 1), (2, 3), (1, 2), (3, 2),
    (2, 2),
]
IDX = {rel: i for i, rel in enumerate(REL)}
GROUPS = [(0, 5), (5, 6), (11, 4), (15, 1)]
ZP, ZM, YP, YM = (1, 0), (3, 0), (0, 1), (0, 3)
N_MSG = 160


def layer_kernel(
    mixed_h, tok_h, wmix_h, gain_h, bg_h, slot_h, rw_h, gate_h, up_h, down_h, eg_h, eu_h, ed_h,
    out,
    ah, tok, wmix, gain, bg, macc, rw, w, d, eg, eu, ed, meta, g, res, hid, xo, xp, xb, xs, eh, el, sb, rsr, rb, eret,
    ssem, rsem, lsem,
):
    me = lax.axis_index("ep")
    x = lax.axis_index("tp")
    c = lax.rem(me, 2)
    zy = lax.div(me, 2)
    y = lax.rem(zy, 4)
    z = lax.div(zy, 4)

    def dev(dz, dy, dx, pc):
        zz = lax.rem(z + dz, 4)
        yy = lax.rem(y + dy, 4)
        cc = 1 - c if pc else c
        return ((zz * 4 + yy) * 2 + cc, lax.rem(x + dx, 4))

    count = [0]
    sent = []

    class Msg:
        def __init__(self, src, dst, device):
            n = count[0]
            count[0] += 1
            self.copy = pltpu.make_async_remote_copy(
                src_ref=src, dst_ref=dst, send_sem=ssem.at[n], recv_sem=rsem.at[n], device_id=device, device_id_type=MESH
            )

        def start(self):
            self.copy.start()
            sent.append(self.copy)
            return self

        def arrived(self):
            self.copy.wait_recv()

    local = []

    def load(src, dst):
        cp = pltpu.make_async_copy(src, dst, lsem.at[len(local)])
        local.append(cp)
        cp.start()
        return cp

    barrier = pltpu.get_barrier_semaphore()
    peers = [dev(0, 0, 1, 0), dev(0, 0, 2, 0), dev(0, 0, 3, 0), dev(0, 0, 0, 1)]
    peers += [dev(dz, dy, 0, 0) for dz, dy in (ZP, ZM, YP, YM, (2, 0), (0, 2))]
    for peer in peers:
        pl.semaphore_signal(barrier, inc=1, device_id=peer, device_id_type=MESH)

    here = y * 4 + z
    cp_mixed = load(mixed_h, ah.at[x])
    cp_slot = load(slot_h, meta.at[here])
    cp_wmix = load(wmix_h, wmix)
    cp_tok = load(tok_h, tok)
    cp_gain = load(gain_h, gain)
    cp_bg = load(bg_h, bg)
    cp_rw = load(rw_h, rw)

    cp_mixed.wait()
    cp_slot.wait()
    pl.semaphore_wait(barrier, len(peers))

    heads = {}
    for dx in (2, 1, 3):
        heads[(4 - dx) % 4] = Msg(ah.at[x], ah.at[x], dev(0, 0, dx, 0)).start()
    m_z = [Msg(meta.at[here], meta.at[here], dev(dz, 0, 0, 0)).start() for dz in (2, 1, 3)]

    cp_gate = load(gate_h, w.at[0:64])
    cp_up = load(up_h, w.at[128:192])
    w_p = [
        Msg(gate_h, w.at[64:128], dev(0, 0, 0, 1)).start(),
        Msg(up_h, w.at[192:256], dev(0, 0, 0, 1)).start(),
    ]
    cols = pl.ds(pl.multiple_of(x * 512, 512), 512)
    cp_down = load(down_h.at[:, cols], d.at[0:64])
    cp_ed = load(ed_h.at[:, cols], ed.at[0:256])
    cp_eg = load(eg_h, eg)
    cp_eu = load(eu_h, eu)
    down_x, ed_x = {}, {}
    for dx in (2, 1, 3):
        their = pl.ds(pl.multiple_of(lax.rem(x + dx, 4) * 512, 512), 512)
        s = (4 - dx) % 4
        down_x[s] = Msg(down_h.at[:, their], d.at[s * 128 : s * 128 + 64], dev(0, 0, dx, 0)).start()
        ed_x[s] = Msg(ed_h.at[:, their], ed.at[s * 256 : s * 256 + 256], dev(0, 0, dx, 0)).start()
    down_p = [Msg(down_h.at[:, cols], d.at[64:128], dev(0, 0, 0, 1)).start()]

    cp_wmix.wait()
    cp_tok.wait()
    cp_gain.wait()
    cp_bg.wait()

    def head_part(s, n):
        src = lax.rem(x + s, 4)
        rows = pl.ds(pl.multiple_of(src * 256, 256), 256)
        return dot(ah[src], wmix[rows, n * 512 : (n + 1) * 512])

    for n in range(4):
        s = slice(n * 512, (n + 1) * 512)
        macc[:, s] = tok[:, s].astype(F32) + head_part(0, n)
    for h in (1, 3):
        heads[h].arrived()
        for n in range(4):
            macc[:, n * 512 : (n + 1) * 512] += head_part(h, n)
    heads[2].arrived()
    sq = jnp.zeros((48, 1), F32)
    for n in range(4):
        s = slice(n * 512, (n + 1) * 512)
        r = (macc[:, s] + head_part(2, n)).astype(BF16)
        res[:, s] = r
        rf = r.astype(F32)
        sq = sq + jnp.sum(rf * rf, axis=-1, keepdims=True)
    inv = lax.rsqrt(sq * (1.0 / 2048.0) + EPS)
    for n in range(4):
        s = slice(n * 512, (n + 1) * 512)
        g[0, n] = (res[:, s].astype(F32) * inv * gain[:, s]).astype(BF16)

    def spread(rel, q0, nq, way):
        to = ((rel[0] - way[0]) % 4, (rel[1] - way[1]) % 4)
        q = pl.ds(q0, nq)
        return Msg(g.at[IDX[rel], q], g.at[IDX[to], q], dev(*way, 0, 0)).start()

    O = (0, 0)
    a_zp, a_zm = spread(O, 0, 2, ZP), spread(O, 0, 2, ZM)
    b_yp, b_ym = spread(O, 2, 2, YP), spread(O, 2, 2, YM)
    for m in m_z:
        m.arrived()
    col = pl.ds(y * 4, 4)
    m_y = [Msg(meta.at[col], meta.at[col], dev(0, dy, 0, 0)).start() for dy in (2, 1, 3)]
    a_yp, a_ym = spread(O, 0, 2, YP), spread(O, 0, 2, YM)
    b_zp, b_zm = spread(O, 2, 2, ZP), spread(O, 2, 2, ZM)

    gate_sum = jnp.zeros((48, 1), F32)
    for n in range(4):
        s = slice(n * 512, (n + 1) * 512)
        gate_sum = gate_sum + jnp.sum(g[0, n].astype(F32) * bg[:, s].astype(F32), axis=-1, keepdims=True)
    bw = jax.nn.sigmoid(gate_sum)
    cp_rw.wait()
    scol = as_columns(meta[here])
    rwc = as_columns(rw[...])

    a_zp.arrived()
    f_z0 = spread((3, 0), 0, 1, ZP)
    t_33, t_31 = spread((3, 0), 0, 2, YP), spread((3, 0), 0, 2, YM)
    a_zm.arrived()
    f_z1 = spread((1, 0), 1, 1, ZM)
    t_13, t_11 = spread((1, 0), 0, 2, YP), spread((1, 0), 0, 2, YM)
    b_yp.arrived()
    f_y2 = spread((0, 3), 2, 1, YP)
    u_33, u_13 = spread((0, 3), 2, 2, ZP), spread((0, 3), 2, 2, ZM)
    b_ym.arrived()
    f_y3 = spread((0, 1), 3, 1, YM)
    u_31, u_11 = spread((0, 1), 2, 2, ZP), spread((0, 1), 2, 2, ZM)
    a_yp.arrived()
    f_y0 = spread((0, 3), 0, 1, YP)
    a_ym.arrived()
    f_y1 = spread((0, 1), 1, 1, YM)
    b_zp.arrived()
    f_z2 = spread((3, 0), 2, 1, ZP)
    b_zm.arrived()
    f_z3 = spread((1, 0), 3, 1, ZM)

    def up_group(n):
        r0, nb = GROUPS[n]
        acc = None
        for q in range(4):
            part = dot_nt(g[r0 : r0 + nb, q].reshape(nb * 48, 512), w[:, q * 512 : (q + 1) * 512])
            acc = part if acc is None else acc + part
        ga, up = acc[:, 0:128], acc[:, 128:256]
        rows = pl.ds(r0 * 48, nb * 48)
        hid[rows, 0:128] = (ga * jax.nn.sigmoid(ga) * up).astype(BF16)
        out = {}
        for dx in (2, 1, 3):
            s = (4 - dx) % 4
            out[s] = Msg(hid.at[rows, 0:128], hid.at[rows, s * 128 : s * 128 + 128], dev(0, 0, dx, 0)).start()
        return out

    e_mine = (me * 16).astype(F32)
    e_other = ((zy * 2 + (1 - c)) * 16).astype(F32)

    def pick_group(n):
        r0, nb = GROUPS[n]
        lane8 = lax.broadcasted_iota(jnp.int32, (8, 48), 0).astype(F32)
        code = jnp.concatenate([lane8 + e_mine, lane8 + e_other], axis=0)
        for r in range(r0, r0 + nb):
            dz, dy = REL[r]
            m = meta[lax.rem(y + dy, 4) * 4 + lax.rem(z + dz, 4)]
            hit = jnp.where(m[0:1, 0:48] == code, 1.0, 0.0) + jnp.where(m[1:2, 0:48] == code, 1.0, 0.0)
            hit = hit.astype(BF16)
            for q in range(4):
                picked = dot(hit, g[r, q])
                s = slice(q * 512, (q + 1) * 512)
                xo[r * 8 : r * 8 + 8, s] = picked[0:8]
                xp[r * 8 : r * 8 + 8, s] = picked[8:16]

    def pass_rows(a, b):
        rows = slice(a, b)
        xs[rows] = xp[rows].astype(BF16)
        return Msg(xs.at[rows], xb.at[rows], dev(0, 0, 0, 1)).start()

    cp_gate.wait()
    cp_up.wait()
    for m in w_p:
        m.arrived()
    hid_in = {}
    hid_in[0] = up_group(0)
    for m in m_y:
        m.arrived()
    pick_group(0)

    f_z0.arrived()
    f_z1.arrived()
    t_23, t_21 = spread((2, 0), 0, 2, YP), spread((2, 0), 0, 2, YM)
    f_y2.arrived()
    f_y3.arrived()
    u_32, u_12 = spread((0, 2), 2, 2, ZP), spread((0, 2), 2, 2, ZM)
    t_33.arrived()
    h_32a = spread((3, 3), 0, 1, YP)
    t_31.arrived()
    h_32b = spread((3, 1), 1, 1, YM)
    t_13.arrived()
    h_12a = spread((1, 3), 0, 1, YP)
    t_11.arrived()
    h_12b = spread((1, 1), 1, 1, YM)
    u_33.arrived()
    h_23a = spread((3, 3), 2, 1, ZP)
    u_13.arrived()
    h_23b = spread((1, 3), 3, 1, ZM)
    u_31.arrived()
    h_21a = spread((3, 1), 2, 1, ZP)
    u_11.arrived()
    h_21b = spread((1, 1), 3, 1, ZM)
    for m in (f_y0, f_y1, f_z2, f_z3):
        m.arrived()

    hid_in[1] = up_group(1)

    t_23.arrived()
    l_22a = spread((2, 3), 0, 1, YP)
    t_21.arrived()
    l_22b = spread((2, 1), 1, 1, YM)
    u_32.arrived()
    l_22c = spread((3, 2), 2, 1, ZP)
    u_12.arrived()
    l_22d = spread((1, 2), 3, 1, ZM)

    cp_down.wait()
    for s in (1, 2, 3):
        down_x[s].arrived()
        own = slice(s * 128, s * 128 + 64)
        down_p.append(Msg(d.at[own], d.at[s * 128 + 64 : s * 128 + 128], dev(0, 0, 0, 1)).start())

    pick_group(1)

    for m in (h_32a, h_32b, h_12a, h_12b, h_23a, h_23b, h_21a, h_21b):
        m.arrived()
    hid_in[2] = up_group(2)
    pick_group(2)
    passed = pass_rows(0, 112)

    reduced = {}

    def down_group(n):
        r0, nb = GROUPS[n]
        for m in hid_in[n].values():
            m.arrived()
        part = dot(hid[r0 * 48 : (r0 + nb) * 48, :], d[...])
        for i in range(nb):
            r = r0 + i
            blk = part[i * 48 : (i + 1) * 48].astype(BF16)
            if r == 0:
                rsr[0] = blk
            else:
                dz, dy = REL[r]
                sb[r] = blk
                back = IDX[((-dz) % 4, (-dy) % 4)]
                reduced[back] = Msg(sb.at[r], rsr.at[back], dev(dz, dy, 0, 0)).start()

    for m in down_p:
        m.arrived()
    down_group(0)

    cp_eg.wait()
    cp_eu.wait()

    def expert_up(rows_in):
        ga = dot(rows_in, eg[...])
        up = dot(rows_in, eu[...])
        return (ga * jax.nn.sigmoid(ga) * up).astype(BF16)

    def send_hidden(ref):
        out = []
        for dx in (2, 1, 3):
            s = (4 - dx) % 4
            out.append(Msg(ref.at[:, 0:256], ref.at[:, s * 256 : s * 256 + 256], dev(0, 0, dx, 0)).start())
        return out

    eh[0, :, 0:256] = expert_up(xo[0:112].astype(BF16))
    eh_in = send_hidden(eh.at[0])
    down_group(1)
    passed.arrived()
    eh[1, :, 0:256] = expert_up(xb[0:112])
    eh_in += send_hidden(eh.at[1])

    for m in (l_22a, l_22b, l_22c, l_22d):
        m.arrived()
    pick_group(3)
    passed = pass_rows(112, 128)
    hid_in[3] = up_group(3)
    down_group(2)
    passed.arrived()
    el[:, 0:256] = expert_up(jnp.concatenate([xo[112:128].astype(BF16), xb[112:128]], axis=0))
    el_in = send_hidden(el)

    cp_ed.wait()
    for m in ed_x.values():
        m.arrived()
    returned = []

    def give_back(half, r, eo):
        blk = jnp.concatenate([eo[:, 0:256], eo[:, 256:512]], axis=0).astype(BF16)
        if r == 0 and half == 0:
            eret[me] = blk
        else:
            dz, dy = REL[r]
            rb[half, r] = blk
            returned.append(Msg(rb.at[half, r], eret.at[me], dev(dz, dy, 0, half)).start())

    for m in eh_in:
        m.arrived()
    eo = dot(eh[...].reshape(224, 1024), ed[...])
    for r in range(13, -1, -1):
        for half in range(2):
            give_back(half, r, eo[half * 112 + r * 8 : half * 112 + r * 8 + 8])
    down_group(3)
    for m in el_in:
        m.arrived()
    eo = dot(el[...], ed[...])
    for r in (15, 14):
        for half in range(2):
            give_back(half, r, eo[half * 16 + (r - 14) * 8 : half * 16 + (r - 14) * 8 + 8])

    lane = lax.broadcasted_iota(jnp.int32, (48, 512), 1).astype(F32)
    sel = jnp.concatenate(
        [jnp.where(lane == scol[0:48, ch : ch + 1] + float(hf * 8), 1.0, 0.0) for hf in range(2) for ch in range(2)], axis=0
    ).astype(BF16)
    total = rsr[0].astype(F32)
    for r in range(1, 16):
        reduced[r].arrived()
        total = total + rsr[r].astype(F32)
    base = res[:, cols].astype(F32) + bw * total
    for m in returned:
        m.arrived()
    got = dot(sel, eret[...].reshape(512, 256))
    for hf in range(2):
        s = slice(hf * 256, hf * 256 + 256)
        first, second = got[hf * 96 : hf * 96 + 48], got[hf * 96 + 48 : hf * 96 + 96]
        out[:, s] = (base[:, s] + first * rwc[0:48, 0:1] + second * rwc[0:48, 1:2]).astype(BF16)

    for cp in sent:
        cp.wait_send()


def layer_call(*args):
    any_ = pl.BlockSpec(memory_space=pl.ANY)
    vm = pl.BlockSpec(memory_space=pltpu.VMEM)
    return pl.pallas_call(
        layer_kernel,
        out_shape=jax.ShapeDtypeStruct((48, 512), BF16),
        in_specs=[any_] * 13,
        out_specs=vm,
        scratch_shapes=[
            pltpu.VMEM((4, 48, 256), BF16),
            pltpu.VMEM((48, 2048), BF16),
            pltpu.VMEM((1024, 2048), BF16),
            pltpu.VMEM((1, 2048), F32),
            pltpu.VMEM((1, 2048), BF16),
            pltpu.VMEM((48, 2048), F32),
            pltpu.VMEM((2, 48), F32),
            pltpu.VMEM((256, 2048), BF16),
            pltpu.VMEM((512, 512), BF16),
            pltpu.VMEM((2048, 256), BF16),
            pltpu.VMEM((2048, 256), BF16),
            pltpu.VMEM((1024, 512), BF16),
            pltpu.VMEM((16, 8, 128), F32),
            pltpu.VMEM((16, 4, 48, 512), BF16),
            pltpu.VMEM((48, 2048), BF16),
            pltpu.VMEM((768, 512), BF16),
            pltpu.VMEM((128, 2048), F32),
            pltpu.VMEM((128, 2048), F32),
            pltpu.VMEM((128, 2048), BF16),
            pltpu.VMEM((128, 2048), BF16),
            pltpu.VMEM((2, 112, 1024), BF16),
            pltpu.VMEM((32, 1024), BF16),
            pltpu.VMEM((16, 48, 512), BF16),
            pltpu.VMEM((16, 48, 512), BF16),
            pltpu.VMEM((2, 16, 16, 256), BF16),
            pltpu.VMEM((32, 16, 256), BF16),
            pltpu.SemaphoreType.DMA((N_MSG,)),
            pltpu.SemaphoreType.DMA((N_MSG,)),
            pltpu.SemaphoreType.DMA((16,)),
        ],
        compiler_params=pltpu.CompilerParams(vmem_limit_bytes=67043328, collective_id=0, has_side_effects=True),
        name="layer",
    )(*args)


def local(
    tokens, mix_gain, w_query, w_key, w_value, w_outgate, w_ingate, w_forget, in_bias, forget_bias, w_mix_out,
    cell_state, norm_state, max_state, moe_gain, route_ids, route_weights, expert_gate, expert_up, expert_down,
    branch_gate, dense_gate, dense_up, dense_down,
):
    mixed, new_cell, new_norm, new_max, slots = cell_call(
        tokens, mix_gain.reshape(1, 2048), w_query, w_key, w_value, w_outgate, w_ingate.T, w_forget.T,
        in_bias, forget_bias, cell_state, norm_state.reshape(96, 128), max_state.T, route_ids.T,
    )
    layer_out = layer_call(
        mixed, tokens, w_mix_out, moe_gain.reshape(1, 2048), branch_gate.reshape(1, 2048), slots, route_weights.T,
        dense_gate.T, dense_up.T, dense_down,
        expert_gate.reshape(2048, 256), expert_up.reshape(2048, 256), expert_down.reshape(256, 2048),
    )
    return (layer_out, new_cell, new_norm.reshape(48, 2, 128), new_max.T)


def solution(mesh):
    in_specs = (
        P("ep", None),
        P(),
        P(None, "tp"),
        P(None, "tp"),
        P(None, "tp"),
        P(None, "tp"),
        P(None, "tp"),
        P(None, "tp"),
        P("tp"),
        P("tp"),
        P(),
        P("ep", "tp", None, None),
        P("ep", "tp", None),
        P("ep", "tp"),
        P(),
        P("ep", None),
        P("ep", None),
        P("ep", None, "tp"),
        P("ep", None, "tp"),
        P("ep", "tp", None),
        P(),
        P(None, ("ep", "tp")),
        P(None, ("ep", "tp")),
        P(("ep", "tp"), None),
    )
    out_specs = (P("ep", "tp"), P("ep", "tp", None, None), P("ep", "tp", None), P("ep", "tp"))
    return jax.shard_map(local, mesh=mesh, in_specs=in_specs, out_specs=out_specs, check_vma=False)
```

time: 82.8 us -> 67.1 us (0.81)
  local copies, waits for them, and re-layouts: 14.9 us -> 2.71 us
  Pallas kernels: 66.5 us -> 63.5 us
    unnamed x49 -> x1, local copies, waits for them, and re-layouts: 14.2 us -> 1.42 us
    pallas_call x1, Pallas kernels: 12.1 us -> 9.33 us  [cell_call(): pl.pallas_call(cell_kernel, out_shape=(jax.ShapeDtypeStruct((48, 256), BF...]
where the time goes in v2:
time: 67.1 us; the launch traced here: 66.9 us
  Pallas kernels  63.5 us (95%)
  local copies, waits for them, and re-layouts  2.71 us (4%)
    pallas_call x1, Pallas kernels, layer_call(): pl.pallas_call(layer_kernel, out_shape=jax.ShapeDtypeStruct((48, 512), BF...  54.2 us
    pallas_call x1, Pallas kernels, cell_call(): pl.pallas_call(cell_kernel, out_shape=(jax.ShapeDtypeStruct((48, 256), BF...  9.33 us
    unnamed x1, local copies, waits for them, and re-layouts  1.42 us

profile of v2, /device:TPU:1, one launch (start us, length us, event | category | flops | bytes accessed | tf_op | source)
XLA Modules:
  0.0 66.9 jit_solution(14337736293482509163)
XLA Ops:
  0.6 1.3 %reshape.35.bg_h = bf16[1,2048]{1,0:T(2,128)(2,1)} reshape(bf16[2048]{0:T(1024)(128)(2,1)} %param.44) | data formatting | bytes 8192 | tf_op jit(solution)/shard_map/reshape | solution.py:644
  1.9 9.3 %cell.1 = (bf16[48,256]{1,0:T(8,128)(2,1)}, f32[48,2,128,128]{3,2,1,0:T(8,128)}, f32[96,128]{1,0:T(8,128)}, f32[2,48]{1,0:T(2,128)}, f32[8,128]{1,0:T(8,128)}) custom-call(bf16[48,2048]{1,0:T(8,128)(2,1)} %tok_h.3, f32[1,2048]{1,0:T(1,128)} %bitcast.22, bf16[2048,256]{1,0:T(8,128)(2,1)} %wq_h.1, bf16[2048,256]{1,0:T(8,128)(2,1)} %wk_h.1, ...), custom_call_target="tpu_custom_call" | custom-call | tf_op jit(solution)/shard_map/cell/pallas_call | solution.py:176
  11.3 54.2 %layer.1 = bf16[48,512]{1,0:T(8,128)(2,1)} custom-call(bf16[48,256]{1,0:T(8,128)(2,1)} %get-tuple-element.9.mixed_h, bf16[48,2048]{1,0:T(8,128)(2,1)} %tok_h.3, bf16[1024,2048]{1,0:T(8,128)(2,1)} %wmix_h.1, f32[1,2048]{1,0:T(1,128)} %bitcast.21, bf16[1,2048]{1,0:T(2,128)(2,1)} %reshape.35.bg_h, f32[8,128]{1,0:T(8,128)} %get-tuple-element.10.slot_h, ...), custom_call_target="tpu_custom_call" | custom-call | tf_op jit(solution)/shard_map/layer/pallas_call | solution.py:593
  65.4 1.4 %copy.29 = bf16[48,512]{1,0:T(8,128)(2,1)} copy(bf16[48,512]{1,0:T(8,128)(2,1)} %layer.1) | data formatting | bytes 98304

commit v3 on v2

v3 whole, which is shorter than its diff:
```python
import functools

import jax
import jax.numpy as jnp
from jax import lax
from jax.experimental import pallas as pl
from jax.experimental.pallas import tpu as pltpu
from jax.sharding import PartitionSpec as P

EPS = 1e-06
MESH = pl.DeviceIdType.MESH
F32 = jnp.float32
BF16 = jnp.bfloat16
NT = (((1,), (1,)), ((), ()))


def dot(a, b):
    return jnp.dot(a, b, preferred_element_type=F32)


def dot_nt(a, b):
    return lax.dot_general(a, b, NT, preferred_element_type=F32)


CHUNK = 6
N_CHUNK = 8


def split3(a):
    first = a.astype(BF16).astype(F32)
    rest = a - first
    second = rest.astype(BF16).astype(F32)
    return first, second, rest - second


def as_columns(rows):
    n, width = rows.shape
    wide = jnp.concatenate([rows, jnp.zeros((n, 128 - width), F32)], axis=1) if width < 128 else rows
    return jnp.concatenate([wide, jnp.zeros((128 - n, 128), F32)], axis=0).T


def slot_rows(ids):
    idf = ids.astype(F32)
    idc = as_columns(idf)
    before = lax.broadcasted_iota(jnp.int32, (48, 48), 0) < lax.broadcasted_iota(jnp.int32, (48, 48), 1)
    slots = []
    for ch in range(2):
        row = idf[ch : ch + 1, :]
        hits = jnp.where(idc[0:48, 0:1] == row, 1.0, 0.0) + jnp.where(idc[0:48, 1:2] == row, 1.0, 0.0)
        rank = jnp.sum(jnp.where(before, hits, 0.0), axis=0, keepdims=True)
        slots.append(row * 16.0 + rank)
    srow = jnp.concatenate(slots + [jnp.zeros((6, 48), F32)], axis=0)
    return jnp.concatenate([srow, jnp.zeros((8, 80), F32)], axis=1)


REL = [
    (0, 0), (1, 0), (3, 0), (0, 1), (0, 3),
    (1, 1), (1, 3), (3, 1), (3, 3), (2, 0), (0, 2),
    (2, 1), (2, 3), (1, 2), (3, 2),
    (2, 2),
]
IDX = {rel: i for i, rel in enumerate(REL)}
GROUPS = [(0, 5), (5, 6), (11, 4), (15, 1)]
ZP, ZM, YP, YM = (1, 0), (3, 0), (0, 1), (0, 3)
N_MSG = 160


def layer_kernel(
    tok_h, cgain_h, wq_h, wk_h, wv_h, wo_h, win_h, wf_h, inb_h, fb_h, cell_h, norm_h, max_h, ids_h,
    wmix_h, gain_h, bg_h, rw_h, gate_h, up_h, down_h, eg_h, eu_h, ed_h,
    out, cell, norm_o, max_o,
    inb, fb, tok, cgain, wts, win, wf, norm, mx, ids, normed, vs, vf, cb, qt, wt, num, wsem, csem, msem,
    ah, wmix, gain, bg, macc, rw, w, d, eg, eu, ed, meta, g, res, hid, xo, xp, xb, xs, eh, el, sb, rsr, rb, eret,
    ssem, rsem, lsem,
):
    me = lax.axis_index("ep")
    x = lax.axis_index("tp")
    c = lax.rem(me, 2)
    zy = lax.div(me, 2)
    y = lax.rem(zy, 4)
    z = lax.div(zy, 4)

    def dev(dz, dy, dx, pc):
        zz = lax.rem(z + dz, 4)
        yy = lax.rem(y + dy, 4)
        cc = 1 - c if pc else c
        return ((zz * 4 + yy) * 2 + cc, lax.rem(x + dx, 4))

    count = [0]
    sent = []

    class Msg:
        def __init__(self, src, dst, device):
            n = count[0]
            count[0] += 1
            self.copy = pltpu.make_async_remote_copy(
                src_ref=src, dst_ref=dst, send_sem=ssem.at[n], recv_sem=rsem.at[n], device_id=device, device_id_type=MESH
            )

        def start(self):
            self.copy.start()
            sent.append(self.copy)
            return self

        def arrived(self):
            self.copy.wait_recv()

    local = []

    def load(src, dst):
        cp = pltpu.make_async_copy(src, dst, lsem.at[len(local)])
        local.append(cp)
        cp.start()
        return cp

    barrier = pltpu.get_barrier_semaphore()
    peers = [dev(0, 0, 1, 0), dev(0, 0, 2, 0), dev(0, 0, 3, 0), dev(0, 0, 0, 1)]
    peers += [dev(dz, dy, 0, 0) for dz, dy in (ZP, ZM, YP, YM, (2, 0), (0, 2))]
    for peer in peers:
        pl.semaphore_signal(barrier, inc=1, device_id=peer, device_id_type=MESH)

    here = y * 4 + z
    cols = pl.ds(pl.multiple_of(x * 512, 512), 512)

    small = [
        pltpu.make_async_copy(src, dst, msem.at[i])
        for i, (src, dst) in enumerate(
            [(tok_h, tok), (cgain_h, cgain), (win_h, win), (wf_h, wf), (max_h, mx), (norm_h, norm), (ids_h, ids), (inb_h, inb), (fb_h, fb)]
        )
    ]
    for cp in small[0:2]:
        cp.start()
    wcp = [pltpu.make_async_copy(src, wts.at[i], wsem.at[i]) for i, src in enumerate([wq_h, wk_h, wv_h, wo_h])]
    wcp[0].start()
    for cp in small[2:]:
        cp.start()
    for cp in wcp[1:]:
        cp.start()

    def cin(i):
        s = pl.ds(i * CHUNK, CHUNK)
        return pltpu.make_async_copy(cell_h.at[s], cell.at[s], csem.at[i])

    for cp in small[0:2]:
        cp.wait()
    for i in range(N_CHUNK):
        cin(i).start()
    xf = tok[...].astype(F32)
    ms = jnp.mean(xf * xf, axis=-1, keepdims=True)
    normed[...] = (xf * lax.rsqrt(ms + EPS) * cgain[...]).astype(BF16)
    nb = normed[...]
    for cp in small[2:]:
        cp.wait()
    meta[here] = slot_rows(ids[...])
    in_pre = dot_nt(win[...], nb)
    fpre = dot_nt(wf[...], nb)
    hrow = lax.broadcasted_iota(jnp.int32, in_pre.shape, 0)
    in_pre = in_pre + jnp.where(hrow == 0, inb[0], inb[1])
    fpre = fpre + jnp.where(hrow == 0, fb[0], fb[1])
    log_f = jnp.minimum(fpre, 0.0) - jnp.log1p(jnp.exp(-jnp.abs(fpre)))
    lm = log_f + mx[...]
    new_max = jnp.maximum(lm, in_pre)
    max_o[...] = new_max
    carry = jnp.exp(lm - new_max)
    write = jnp.exp(in_pre - new_max)
    floor = jnp.exp(-new_max)
    rows = jnp.concatenate([carry, write, floor], axis=0)
    rows = jnp.concatenate([rows, jnp.zeros((6, 80), F32)], axis=1)
    rows = jnp.concatenate([rows, jnp.zeros((122, 128), F32)], axis=0)
    gcols = rows.T

    wcp[0].wait()
    q = dot(nb, wts[0])
    wcp[1].wait()
    k = dot(nb, wts[1]) * (128 ** (-0.5))
    wcp[2].wait()
    v = dot(nb, wts[2])
    for h in range(2):
        v1, v2, _ = split3(v[:, h * 128 : (h + 1) * 128])
        vs[h] = jnp.concatenate([v1, v1, v2], axis=0).astype(BF16)
        vf[h] = v[:, h * 128 : (h + 1) * 128]
    cp_wmix = load(wmix_h, wmix)
    cp_gain = load(gain_h, gain)
    cp_bg = load(bg_h, bg)
    cp_rw = load(rw_h, rw)
    cp_gate = load(gate_h, w.at[0:64])
    cp_up = load(up_h, w.at[128:192])
    cp_down = load(down_h.at[:, cols], d.at[0:64])
    cp_ed = load(ed_h.at[:, cols], ed.at[0:256])
    cp_eg = load(eg_h, eg)
    cp_eu = load(eu_h, eu)
    wcp[3].wait()
    og = jax.nn.sigmoid(dot(nb, wts[3]))

    pl.semaphore_wait(barrier, len(peers))
    w_p = [
        Msg(gate_h, w.at[64:128], dev(0, 0, 0, 1)).start(),
        Msg(up_h, w.at[192:256], dev(0, 0, 0, 1)).start(),
    ]
    down_p = [Msg(down_h.at[:, cols], d.at[64:128], dev(0, 0, 0, 1)).start()]
    down_x, ed_x = {}, {}

    def their(dx):
        return pl.ds(pl.multiple_of(lax.rem(x + dx, 4) * 512, 512), 512)

    def send_ed(dx):
        s = (4 - dx) % 4
        ed_x[s] = Msg(ed_h.at[:, their(dx)], ed.at[s * 256 : s * 256 + 256], dev(0, 0, dx, 0)).start()

    for dx in (2, 1, 3):
        s = (4 - dx) % 4
        down_x[s] = Msg(down_h.at[:, their(dx)], d.at[s * 128 : s * 128 + 64], dev(0, 0, dx, 0)).start()

    m_z = [Msg(meta.at[here], meta.at[here], dev(dz, 0, 0, 0)).start() for dz in (2, 1, 3)]

    denom = []
    pad = jnp.zeros((112, 128), F32)
    for h in range(2):
        ca = jnp.broadcast_to(gcols[0:48, h : h + 1], (48, 128))
        wr = jnp.broadcast_to(gcols[0:48, 2 + h : 3 + h], (48, 128))
        qh = q[:, h * 128 : (h + 1) * 128]
        written = wr * k[:, h * 128 : (h + 1) * 128]
        hs = pl.ds(h, 48, stride=2)
        nn = ca * norm[hs, :] + written
        norm_o[hs, :] = nn
        den = jnp.sum(qh * nn, axis=-1, keepdims=True)
        denom.append(jnp.maximum(jnp.abs(den), gcols[0:48, 4 + h : 5 + h]))
        cb[h] = ca
        vf[h] = jnp.sum(qh * written, axis=-1, keepdims=True) * vf[h]
        q1, q2, q3 = split3(qh)
        qt[h] = jnp.concatenate([q1, q2, q3, pad], axis=0).T[:, 0:144].astype(BF16)
        w1, w2, _ = split3(written)
        wt[h] = jnp.concatenate([w1, w2, w1, pad], axis=0).T[:, 0:144].astype(BF16)

    token = lax.rem(lax.broadcasted_iota(jnp.int32, (144, 128), 0), 48)

    def tokens_of(i):
        return [token == i * CHUNK + j for j in range(CHUNK)]

    def read_step(i, _):
        cin(i).wait()
        ones = jnp.concatenate([jnp.where(m, 1.0, 0.0) for m in tokens_of(i)], axis=1).astype(BF16)
        for h in range(2):
            qcols = dot(qt[h], ones)
            for j in range(CHUNK):
                b = i * CHUNK + j
                num[h, pl.ds(b, 1), :] = jnp.sum(
                    qcols[:, j * 128 : (j + 1) * 128] * cell[b, h], axis=0, keepdims=True
                )
        return 0

    def write_step(i, _):
        here = tokens_of(i)
        for h in range(2):
            vh = vs[h].astype(F32)
            vrows = jnp.concatenate([jnp.where(m, vh, 0.0) for m in here], axis=1).astype(BF16)
            outer = dot(wt[h], vrows)
            for j in range(CHUNK):
                b = i * CHUNK + j
                cell[b, h] = cb[h, pl.ds(b, 1), :] * cell[b, h] + outer[:, j * 128 : (j + 1) * 128]
        return 0

    lax.fori_loop(0, N_CHUNK, read_step, 0)
    for h in range(2):
        lanes = slice(h * 128, (h + 1) * 128)
        ah[x, :, lanes] = (og[:, lanes] * ((cb[h] * num[h] + vf[h]) / denom[h])).astype(BF16)

    heads = {}
    for dx in (2, 1, 3):
        heads[(4 - dx) % 4] = Msg(ah.at[x], ah.at[x], dev(0, 0, dx, 0)).start()

    cp_wmix.wait()
    cp_gain.wait()
    cp_bg.wait()

    def head_part(s, n):
        src = lax.rem(x + s, 4)
        rows = pl.ds(pl.multiple_of(src * 256, 256), 256)
        return dot(ah[src], wmix[rows, n * 512 : (n + 1) * 512])

    for n in range(4):
        s = slice(n * 512, (n + 1) * 512)
        macc[:, s] = tok[:, s].astype(F32) + head_part(0, n)
    for h in (1, 3):
        heads[h].arrived()
        for n in range(4):
            macc[:, n * 512 : (n + 1) * 512] += head_part(h, n)
    heads[2].arrived()
    sq = jnp.zeros((48, 1), F32)
    for n in range(4):
        s = slice(n * 512, (n + 1) * 512)
        r = (macc[:, s] + head_part(2, n)).astype(BF16)
        res[:, s] = r
        rf = r.astype(F32)
        sq = sq + jnp.sum(rf * rf, axis=-1, keepdims=True)
    inv = lax.rsqrt(sq * (1.0 / 2048.0) + EPS)
    for n in range(4):
        s = slice(n * 512, (n + 1) * 512)
        g[0, n] = (res[:, s].astype(F32) * inv * gain[:, s]).astype(BF16)

    def spread(rel, q0, nq, way):
        to = ((rel[0] - way[0]) % 4, (rel[1] - way[1]) % 4)
        q = pl.ds(q0, nq)
        return Msg(g.at[IDX[rel], q], g.at[IDX[to], q], dev(*way, 0, 0)).start()

    O = (0, 0)
    a_zp, a_zm = spread(O, 0, 2, ZP), spread(O, 0, 2, ZM)
    b_yp, b_ym = spread(O, 2, 2, YP), spread(O, 2, 2, YM)
    for m in m_z:
        m.arrived()
    col = pl.ds(y * 4, 4)
    m_y = [Msg(meta.at[col], meta.at[col], dev(0, dy, 0, 0)).start() for dy in (2, 1, 3)]
    a_yp, a_ym = spread(O, 0, 2, YP), spread(O, 0, 2, YM)
    b_zp, b_zm = spread(O, 2, 2, ZP), spread(O, 2, 2, ZM)

    for dx in (2, 1, 3):
        send_ed(dx)

    lax.fori_loop(0, N_CHUNK, write_step, 0)

    gate_sum = jnp.zeros((48, 1), F32)
    gate_rows = bg[...].astype(F32)
    for n in range(4):
        rowsum = jnp.zeros((48, 128), F32)
        for i in range(4):
            rowsum = rowsum + g[0, n, :, i * 128 : (i + 1) * 128].astype(F32) * gate_rows[n * 4 + i : n * 4 + i + 1]
        gate_sum = gate_sum + jnp.sum(rowsum, axis=-1, keepdims=True)
    bw = jax.nn.sigmoid(gate_sum)
    cp_rw.wait()
    scol = as_columns(meta[here])
    rwc = as_columns(rw[...])

    a_zp.arrived()
    f_z0 = spread((3, 0), 0, 1, ZP)
    t_33, t_31 = spread((3, 0), 0, 2, YP), spread((3, 0), 0, 2, YM)
    a_zm.arrived()
    f_z1 = spread((1, 0), 1, 1, ZM)
    t_13, t_11 = spread((1, 0), 0, 2, YP), spread((1, 0), 0, 2, YM)
    b_yp.arrived()
    f_y2 = spread((0, 3), 2, 1, YP)
    u_33, u_13 = spread((0, 3), 2, 2, ZP), spread((0, 3), 2, 2, ZM)
    b_ym.arrived()
    f_y3 = spread((0, 1), 3, 1, YM)
    u_31, u_11 = spread((0, 1), 2, 2, ZP), spread((0, 1), 2, 2, ZM)
    a_yp.arrived()
    f_y0 = spread((0, 3), 0, 1, YP)
    a_ym.arrived()
    f_y1 = spread((0, 1), 1, 1, YM)
    b_zp.arrived()
    f_z2 = spread((3, 0), 2, 1, ZP)
    b_zm.arrived()
    f_z3 = spread((1, 0), 3, 1, ZM)

    def up_group(n):
        r0, nb = GROUPS[n]
        acc = None
        for q in range(4):
            part = dot_nt(g[r0 : r0 + nb, q].reshape(nb * 48, 512), w[:, q * 512 : (q + 1) * 512])
            acc = part if acc is None else acc + part
        ga, up = acc[:, 0:128], acc[:, 128:256]
        rows = pl.ds(r0 * 48, nb * 48)
        hid[rows, 0:128] = (ga * jax.nn.sigmoid(ga) * up).astype(BF16)
        out = {}
        for dx in (2, 1, 3):
            s = (4 - dx) % 4
            out[s] = Msg(hid.at[rows, 0:128], hid.at[rows, s * 128 : s * 128 + 128], dev(0, 0, dx, 0)).start()
        return out

    e_mine = (me * 16).astype(F32)
    e_other = ((zy * 2 + (1 - c)) * 16).astype(F32)

    def pick_group(n):
        r0, nb = GROUPS[n]
        lane8 = lax.broadcasted_iota(jnp.int32, (8, 48), 0).astype(F32)
        code = jnp.concatenate([lane8 + e_mine, lane8 + e_other], axis=0)
        for r in range(r0, r0 + nb):
            dz, dy = REL[r]
            m = meta[lax.rem(y + dy, 4) * 4 + lax.rem(z + dz, 4)]
            hit = jnp.where(m[0:1, 0:48] == code, 1.0, 0.0) + jnp.where(m[1:2, 0:48] == code, 1.0, 0.0)
            hit = hit.astype(BF16)
            for q in range(4):
                picked = dot(hit, g[r, q])
                s = slice(q * 512, (q + 1) * 512)
                xo[r * 8 : r * 8 + 8, s] = picked[0:8]
                xp[r * 8 : r * 8 + 8, s] = picked[8:16]

    def pass_rows(a, b):
        rows = slice(a, b)
        xs[rows] = xp[rows].astype(BF16)
        return Msg(xs.at[rows], xb.at[rows], dev(0, 0, 0, 1)).start()

    cp_down.wait()
    for s in (1, 2, 3):
        down_x[s].arrived()
        own = slice(s * 128, s * 128 + 64)
        down_p.append(Msg(d.at[own], d.at[s * 128 + 64 : s * 128 + 128], dev(0, 0, 0, 1)).start())

    cp_gate.wait()
    cp_up.wait()
    for m in w_p:
        m.arrived()
    hid_in = {}
    hid_in[0] = up_group(0)
    for m in m_y:
        m.arrived()
    pick_group(0)

    f_z0.arrived()
    f_z1.arrived()
    t_23, t_21 = spread((2, 0), 0, 2, YP), spread((2, 0), 0, 2, YM)
    f_y2.arrived()
    f_y3.arrived()
    u_32, u_12 = spread((0, 2), 2, 2, ZP), spread((0, 2), 2, 2, ZM)
    t_33.arrived()
    h_32a = spread((3, 3), 0, 1, YP)
    t_31.arrived()
    h_32b = spread((3, 1), 1, 1, YM)
    t_13.arrived()
    h_12a = spread((1, 3), 0, 1, YP)
    t_11.arrived()
    h_12b = spread((1, 1), 1, 1, YM)
    u_33.arrived()
    h_23a = spread((3, 3), 2, 1, ZP)
    u_13.arrived()
    h_23b = spread((1, 3), 3, 1, ZM)
    u_31.arrived()
    h_21a = spread((3, 1), 2, 1, ZP)
    u_11.arrived()
    h_21b = spread((1, 1), 3, 1, ZM)
    for m in (f_y0, f_y1, f_z2, f_z3):
        m.arrived()

    hid_in[1] = up_group(1)

    t_23.arrived()
    l_22a = spread((2, 3), 0, 1, YP)
    t_21.arrived()
    l_22b = spread((2, 1), 1, 1, YM)
    u_32.arrived()
    l_22c = spread((3, 2), 2, 1, ZP)
    u_12.arrived()
    l_22d = spread((1, 2), 3, 1, ZM)

    reduced = {}

    def down_group(n):
        r0, nb = GROUPS[n]
        for m in hid_in[n].values():
            m.arrived()
        part = dot(hid[r0 * 48 : (r0 + nb) * 48, :], d[...])
        for i in range(nb):
            r = r0 + i
            blk = part[i * 48 : (i + 1) * 48].astype(BF16)
            if r == 0:
                rsr[0] = blk
            else:
                dz, dy = REL[r]
                sb[r] = blk
                back = IDX[((-dz) % 4, (-dy) % 4)]
                reduced[back] = Msg(sb.at[r], rsr.at[back], dev(dz, dy, 0, 0)).start()

    pick_group(1)
    first_rows = pass_rows(0, 80)
    for m in down_p:
        m.arrived()
    down_group(0)
    for m in (h_32a, h_32b, h_12a, h_12b, h_23a, h_23b, h_21a, h_21b):
        m.arrived()
    hid_in[2] = up_group(2)
    pick_group(2)
    passed = [pass_rows(80, 112)]
    down_group(1)

    cp_eg.wait()
    cp_eu.wait()

    def expert_up(ref, a, b):
        rows_in = jnp.concatenate([xo[a:b].astype(BF16), xb[a:b]], axis=0)
        ga = dot(rows_in, eg[...])
        up = dot(rows_in, eu[...])
        ref[:, 0:256] = (ga * jax.nn.sigmoid(ga) * up).astype(BF16)
        out = []
        for dx in (2, 1, 3):
            s = (4 - dx) % 4
            out.append(Msg(ref.at[:, 0:256], ref.at[:, s * 256 : s * 256 + 256], dev(0, 0, dx, 0)).start())
        return out

    first_rows.arrived()
    eh_in = expert_up(eh, 0, 80)

    for m in (l_22a, l_22b, l_22c, l_22d):
        m.arrived()
    pick_group(3)
    passed.append(pass_rows(112, 128))
    hid_in[3] = up_group(3)
    for m in passed:
        m.arrived()
    el_in = expert_up(el, 80, 128)
    down_group(2)
    down_group(3)

    cp_ed.wait()
    for m in ed_x.values():
        m.arrived()
    returned = []

    def give_back(half, r, eo):
        blk = jnp.concatenate([eo[:, 0:256], eo[:, 256:512]], axis=0).astype(BF16)
        if r == 0 and half == 0:
            eret[me] = blk
        else:
            dz, dy = REL[r]
            rb[half, r] = blk
            returned.append(Msg(rb.at[half, r], eret.at[me], dev(dz, dy, 0, half)).start())

    for m in eh_in:
        m.arrived()
    eo = dot(eh[...], ed[...])
    for r in range(9, -1, -1):
        for half in range(2):
            give_back(half, r, eo[half * 80 + r * 8 : half * 80 + r * 8 + 8])
    for m in el_in:
        m.arrived()
    eo = dot(el[...], ed[...])
    for r in range(15, 9, -1):
        for half in range(2):
            give_back(half, r, eo[half * 48 + (r - 10) * 8 : half * 48 + (r - 10) * 8 + 8])

    lane = lax.broadcasted_iota(jnp.int32, (48, 512), 1).astype(F32)
    sel = jnp.concatenate(
        [jnp.where(lane == scol[0:48, ch : ch + 1] + float(hf * 8), 1.0, 0.0) for hf in range(2) for ch in range(2)], axis=0
    ).astype(BF16)
    total = rsr[0].astype(F32)
    for r in range(1, 16):
        reduced[r].arrived()
        total = total + rsr[r].astype(F32)
    base = res[:, cols].astype(F32) + bw * total
    for m in returned:
        m.arrived()
    got = dot(sel, eret[...].reshape(512, 256))
    for hf in range(2):
        s = slice(hf * 256, hf * 256 + 256)
        first, second = got[hf * 96 : hf * 96 + 48], got[hf * 96 + 48 : hf * 96 + 96]
        out[:, s] = (base[:, s] + first * rwc[0:48, 0:1] + second * rwc[0:48, 1:2]).astype(BF16)

    for cp in sent:
        cp.wait_send()


def layer_call(*args):
    vm = pl.BlockSpec(memory_space=pltpu.VMEM)
    args = [pltpu.with_memory_space_constraint(a, pltpu.HBM) for a in args]
    return pl.pallas_call(
        layer_kernel,
        out_shape=(
            jax.ShapeDtypeStruct((48, 512), BF16),
            jax.ShapeDtypeStruct((48, 2, 128, 128), F32),
            jax.ShapeDtypeStruct((96, 128), F32),
            jax.ShapeDtypeStruct((2, 48), F32),
        ),
        in_specs=[pl.BlockSpec(memory_space=pltpu.HBM)] * 24,
        out_specs=(vm, vm, vm, vm),
        scratch_shapes=[
            pltpu.SMEM((2,), F32),
            pltpu.SMEM((2,), F32),
            pltpu.VMEM((48, 2048), BF16),
            pltpu.VMEM((1, 2048), F32),
            pltpu.VMEM((4, 2048, 256), BF16),
            pltpu.VMEM((2, 2048), BF16),
            pltpu.VMEM((2, 2048), BF16),
            pltpu.VMEM((96, 128), F32),
            pltpu.VMEM((2, 48), F32),
            pltpu.VMEM((2, 48), jnp.int32),
            pltpu.VMEM((48, 2048), BF16),
            pltpu.VMEM((2, 144, 128), BF16),
            pltpu.VMEM((2, 48, 128), F32),
            pltpu.VMEM((2, 48, 128), F32),
            pltpu.VMEM((2, 128, 144), BF16),
            pltpu.VMEM((2, 128, 144), BF16),
            pltpu.VMEM((2, 48, 128), F32),
            pltpu.SemaphoreType.DMA((4,)),
            pltpu.SemaphoreType.DMA((N_CHUNK,)),
            pltpu.SemaphoreType.DMA((9,)),
            pltpu.VMEM((4, 48, 256), BF16),
            pltpu.VMEM((1024, 2048), BF16),
            pltpu.VMEM((1, 2048), F32),
            pltpu.VMEM((16, 128), BF16),
            pltpu.VMEM((48, 2048), F32),
            pltpu.VMEM((2, 48), F32),
            pltpu.VMEM((256, 2048), BF16),
            pltpu.VMEM((512, 512), BF16),
            pltpu.VMEM((2048, 256), BF16),
            pltpu.VMEM((2048, 256), BF16),
            pltpu.VMEM((1024, 512), BF16),
            pltpu.VMEM((16, 8, 128), F32),
            pltpu.VMEM((16, 4, 48, 512), BF16),
            pltpu.VMEM((48, 2048), BF16),
            pltpu.VMEM((768, 512), BF16),
            pltpu.VMEM((128, 2048), F32),
            pltpu.VMEM((128, 2048), F32),
            pltpu.VMEM((128, 2048), BF16),
            pltpu.VMEM((128, 2048), BF16),
            pltpu.VMEM((160, 1024), BF16),
            pltpu.VMEM((96, 1024), BF16),
            pltpu.VMEM((16, 48, 512), BF16),
            pltpu.VMEM((16, 48, 512), BF16),
            pltpu.VMEM((2, 16, 16, 256), BF16),
            pltpu.VMEM((32, 16, 256), BF16),
            pltpu.SemaphoreType.DMA((N_MSG,)),
            pltpu.SemaphoreType.DMA((N_MSG,)),
            pltpu.SemaphoreType.DMA((16,)),
        ],
        compiler_params=pltpu.CompilerParams(vmem_limit_bytes=44 * 2**20, collective_id=0, has_side_effects=True),
        name="layer",
    )(*args)


def finish_kernel(lay, cell, norm, mx, lay_o, cell_o, norm_o, max_o, sem):
    copies = [
        pltpu.make_async_copy(cell.at[12 * i : 12 * i + 12], cell_o.at[12 * i : 12 * i + 12], sem.at[i]) for i in range(4)
    ]
    copies.append(pltpu.make_async_copy(lay, lay_o, sem.at[4]))
    copies.append(pltpu.make_async_copy(norm, norm_o, sem.at[5]))
    copies.append(pltpu.make_async_copy(mx, max_o, sem.at[6]))
    for cp in copies:
        cp.start()
    for cp in copies:
        cp.wait()


def finish_call(*args):
    any_ = pl.BlockSpec(memory_space=pl.ANY)
    vm = pl.BlockSpec(memory_space=pltpu.VMEM)
    return pl.pallas_call(
        finish_kernel,
        out_shape=tuple(jax.ShapeDtypeStruct(a.shape, a.dtype) for a in args),
        in_specs=[vm] * 4,
        out_specs=[any_] * 4,
        scratch_shapes=[pltpu.SemaphoreType.DMA((7,))],
        compiler_params=pltpu.CompilerParams(vmem_limit_bytes=16 * 2**20),
        name="finish",
    )(*[pltpu.with_memory_space_constraint(a, pltpu.VMEM) for a in args])


def local(
    tokens, mix_gain, w_query, w_key, w_value, w_outgate, w_ingate, w_forget, in_bias, forget_bias, w_mix_out,
    cell_state, norm_state, max_state, moe_gain, route_ids, route_weights, expert_gate, expert_up, expert_down,
    branch_gate, dense_gate, dense_up, dense_down,
):
    parts = layer_call(
        tokens, mix_gain.reshape(1, 2048), w_query, w_key, w_value, w_outgate, w_ingate.T, w_forget.T,
        in_bias, forget_bias, cell_state, norm_state.reshape(96, 128), max_state.T, route_ids.T,
        w_mix_out, moe_gain.reshape(1, 2048), branch_gate.reshape(16, 128), route_weights.T,
        dense_gate.T, dense_up.T, dense_down,
        expert_gate.reshape(2048, 256), expert_up.reshape(2048, 256), expert_down.reshape(256, 2048),
    )
    layer_out, new_cell, new_norm, new_max = finish_call(*parts)
    return (layer_out, new_cell, new_norm.reshape(48, 2, 128), new_max.T)


def solution(mesh):
    in_specs = (
        P("ep", None),
        P(),
        P(None, "tp"),
        P(None, "tp"),
        P(None, "tp"),
        P(None, "tp"),
        P(None, "tp"),
        P(None, "tp"),
        P("tp"),
        P("tp"),
        P(),
        P("ep", "tp", None, None),
        P("ep", "tp", None),
        P("ep", "tp"),
        P(),
        P("ep", None),
        P("ep", None),
        P("ep", None, "tp"),
        P("ep", None, "tp"),
        P("ep", "tp", None),
        P(),
        P(None, ("ep", "tp")),
        P(None, ("ep", "tp")),
        P(("ep", "tp"), None),
    )
    out_specs = (P("ep", "tp"), P("ep", "tp", None, None), P("ep", "tp", None), P("ep", "tp"))
    return jax.shard_map(local, mesh=mesh, in_specs=in_specs, out_specs=out_specs, check_vma=False)
```

time: 67.1 us -> 59.5 us (0.89)
  Pallas kernels: 63.5 us -> 58.7 us
  local copies, waits for them, and re-layouts: 2.71 us -> 0 us
    pallas_call x2, Pallas kernels: 63.5 us -> 58.7 us  [the longest x1 56 us: layer_call(): pl.pallas_call(layer_kernel, out_shape=(jax.ShapeDtypeStruct((48, 512), B...]
    unnamed x1 -> x0, local copies, waits for them, and re-layouts: 1.42 us -> none
    reshape x1 -> x0, local copies, waits for them, and re-layouts: 1.29 us -> none  [local(): branch_gate.reshape(1, 2048)]
where the time goes in v3:
time: 59.5 us; the launch traced here: 59.4 us
  Pallas kernels  58.7 us (99%)
  between operations  0.65 us (1%)
    pallas_call x1, Pallas kernels, layer_call(): pl.pallas_call(layer_kernel, out_shape=(jax.ShapeDtypeStruct((48, 512), B...  56 us
    pallas_call x1, Pallas kernels, finish_call(): pl.pallas_call(finish_kernel, out_shape=tuple((jax.ShapeDtypeStruct(a.sha...  2.77 us

profile of v3, /device:TPU:1, one launch (start us, length us, event | category | flops | bytes accessed | tf_op | source)
XLA Modules:
  0.0 59.4 jit_solution(13655840015591142803)
XLA Ops:
  0.6 56.0 %layer.1 = (bf16[48,512]{1,0:T(8,128)(2,1)S(1)}, f32[48,2,128,128]{3,2,1,0:T(8,128)S(1)}, f32[96,128]{1,0:T(8,128)S(1)}, f32[2,48]{1,0:T(2,128)S(1)}) custom-call(bf16[48,2048]{1,0:T(8,128)(2,1)} %tok_h.1, f32[1,2048]{1,0:T(1,128)} %bitcast.22, bf16[2048,256]{1,0:T(8,128)(2,1)} %wq_h.1, bf16[2048,256]{1,0:T(8,128)(2,1)} %wk_h.1, bf16[2048,256]{1,0:T(8,128)(2,1)} %wv_h.1, ...), custom_call_target="tpu_custom_call" | custom-call | tf_op jit(solution)/shard_map/layer/pallas_call | solution.py:553
  56.6 2.8 %finish.1 = (bf16[48,512]{1,0:T(8,128)(2,1)}, f32[48,2,128,128]{3,2,1,0:T(8,128)}, f32[96,128]{1,0:T(8,128)}, f32[2,48]{1,0:T(2,128)}) custom-call(bf16[48,512]{1,0:T(8,128)(2,1)S(1)} %get-tuple-element.12.lay, f32[48,2,128,128]{3,2,1,0:T(8,128)S(1)} %get-tuple-element.13.cell, f32[96,128]{1,0:T(8,128)S(1)} %get-tuple-element.14.norm, ...), custom_call_target="tpu_custom_call" | custom-call | tf_op jit(solution)/shard_map/finish/pallas_call | solution.py:634

commit v4 on v3

--- a/solution.py
+++ b/solution.py
@@ -22,8 +22,8 @@
     return lax.dot_general(a, b, NT, preferred_element_type=F32)
 
 
-CHUNK = 6
-N_CHUNK = 8
+CHUNK = 12
+N_CHUNK = 4
 
 
 def split3(a):
@@ -70,7 +70,7 @@
     wmix_h, gain_h, bg_h, rw_h, gate_h, up_h, down_h, eg_h, eu_h, ed_h,
     out, cell, norm_o, max_o,
     inb, fb, tok, cgain, wts, win, wf, norm, mx, ids, normed, vs, vf, cb, qt, wt, num, wsem, csem, msem,
-    ah, wmix, gain, bg, macc, rw, w, d, eg, eu, ed, meta, g, res, hid, xo, xp, xb, xs, eh, el, sb, rsr, rb, eret,
+    ah, wmix, gain, bg, macc, rw, w, d, eg, eu, ed, meta, g, res, hid, xo, xp, xb, xs, xl, eh, el, ef, sb, rsr, rb, eret,
     ssem, rsem, lsem,
 ):
     me = lax.axis_index("ep")
@@ -169,16 +169,17 @@
     rows = jnp.concatenate([rows, jnp.zeros((122, 128), F32)], axis=0)
     gcols = rows.T
 
-    wcp[0].wait()
+    for cp in wcp:
+        cp.wait()
     q = dot(nb, wts[0])
-    wcp[1].wait()
     k = dot(nb, wts[1]) * (128 ** (-0.5))
-    wcp[2].wait()
     v = dot(nb, wts[2])
     for h in range(2):
         v1, v2, _ = split3(v[:, h * 128 : (h + 1) * 128])
         vs[h] = jnp.concatenate([v1, v1, v2], axis=0).astype(BF16)
         vf[h] = v[:, h * 128 : (h + 1) * 128]
+    og = jax.nn.sigmoid(dot(nb, wts[3]))
+
     cp_wmix = load(wmix_h, wmix)
     cp_gain = load(gain_h, gain)
     cp_bg = load(bg_h, bg)
@@ -189,8 +190,6 @@
     cp_ed = load(ed_h.at[:, cols], ed.at[0:256])
     cp_eg = load(eg_h, eg)
     cp_eu = load(eu_h, eu)
-    wcp[3].wait()
-    og = jax.nn.sigmoid(dot(nb, wts[3]))
 
     pl.semaphore_wait(barrier, len(peers))
     w_p = [
@@ -206,10 +205,6 @@
     def send_ed(dx):
         s = (4 - dx) % 4
         ed_x[s] = Msg(ed_h.at[:, their(dx)], ed.at[s * 256 : s * 256 + 256], dev(0, 0, dx, 0)).start()
-
-    for dx in (2, 1, 3):
-        s = (4 - dx) % 4
-        down_x[s] = Msg(down_h.at[:, their(dx)], d.at[s * 128 : s * 128 + 64], dev(0, 0, dx, 0)).start()
 
     m_z = [Msg(meta.at[here], meta.at[here], dev(dz, 0, 0, 0)).start() for dz in (2, 1, 3)]
 
@@ -314,9 +309,12 @@
     b_zp, b_zm = spread(O, 2, 2, ZP), spread(O, 2, 2, ZM)
 
     for dx in (2, 1, 3):
+        s = (4 - dx) % 4
+        down_x[s] = Msg(down_h.at[:, their(dx)], d.at[s * 128 : s * 128 + 64], dev(0, 0, dx, 0)).start()
+    for dx in (2, 1, 3):
         send_ed(dx)
 
-    lax.fori_loop(0, N_CHUNK, write_step, 0)
+    lax.fori_loop(0, N_CHUNK // 2, write_step, 0)
 
     gate_sum = jnp.zeros((48, 1), F32)
     gate_rows = bg[...].astype(F32)
@@ -381,8 +379,15 @@
             for q in range(4):
                 picked = dot(hit, g[r, q])
                 s = slice(q * 512, (q + 1) * 512)
-                xo[r * 8 : r * 8 + 8, s] = picked[0:8]
-                xp[r * 8 : r * 8 + 8, s] = picked[8:16]
+                if r == 15:
+                    xl[0, :, s] = picked[0:8]
+                    xl[1, :, s] = picked[8:16]
+                else:
+                    xo[r * 6 : r * 6 + 6, s] = picked[0:6]
+                    xp[r * 6 : r * 6 + 6, s] = picked[8:14]
+
+    xo[88:96, :] = jnp.zeros((8, 2048), F32)
+    xp[88:96, :] = jnp.zeros((8, 2048), F32)
 
     def pass_rows(a, b):
         rows = slice(a, b)
@@ -404,6 +409,7 @@
     for m in m_y:
         m.arrived()
     pick_group(0)
+    lax.fori_loop(N_CHUNK // 2, N_CHUNK, write_step, 0)
 
     f_z0.arrived()
     f_z1.arrived()
@@ -430,17 +436,6 @@
     for m in (f_y0, f_y1, f_z2, f_z3):
         m.arrived()
 
-    hid_in[1] = up_group(1)
-
-    t_23.arrived()
-    l_22a = spread((2, 3), 0, 1, YP)
-    t_21.arrived()
-    l_22b = spread((2, 1), 1, 1, YM)
-    u_32.arrived()
-    l_22c = spread((3, 2), 2, 1, ZP)
-    u_12.arrived()
-    l_22d = spread((1, 2), 3, 1, ZM)
-
     reduced = {}
 
     def down_group(n):
@@ -459,23 +454,29 @@
                 back = IDX[((-dz) % 4, (-dy) % 4)]
                 reduced[back] = Msg(sb.at[r], rsr.at[back], dev(dz, dy, 0, 0)).start()
 
+    hid_in[1] = up_group(1)
+
+    t_23.arrived()
+    l_22a = spread((2, 3), 0, 1, YP)
+    t_21.arrived()
+    l_22b = spread((2, 1), 1, 1, YM)
+    u_32.arrived()
+    l_22c = spread((3, 2), 2, 1, ZP)
+    u_12.arrived()
+    l_22d = spread((1, 2), 3, 1, ZM)
+
     pick_group(1)
-    first_rows = pass_rows(0, 80)
-    for m in down_p:
-        m.arrived()
-    down_group(0)
+    first_rows = pass_rows(0, 48)
     for m in (h_32a, h_32b, h_12a, h_12b, h_23a, h_23b, h_21a, h_21b):
         m.arrived()
     hid_in[2] = up_group(2)
     pick_group(2)
-    passed = [pass_rows(80, 112)]
-    down_group(1)
+    second_rows = pass_rows(48, 96)
 
     cp_eg.wait()
     cp_eu.wait()
 
-    def expert_up(ref, a, b):
-        rows_in = jnp.concatenate([xo[a:b].astype(BF16), xb[a:b]], axis=0)
+    def expert_up(ref, rows_in):
         ga = dot(rows_in, eg[...])
         up = dot(rows_in, eu[...])
         ref[:, 0:256] = (ga * jax.nn.sigmoid(ga) * up).astype(BF16)
@@ -486,17 +487,23 @@
         return out
 
     first_rows.arrived()
-    eh_in = expert_up(eh, 0, 80)
+    eh_in = expert_up(eh, jnp.concatenate([xo[0:48].astype(BF16), xb[0:48]], axis=0))
+    for m in down_p:
+        m.arrived()
+    down_group(0)
 
     for m in (l_22a, l_22b, l_22c, l_22d):
         m.arrived()
     pick_group(3)
-    passed.append(pass_rows(112, 128))
+    last_rows = Msg(xl.at[1], xl.at[2], dev(0, 0, 0, 1)).start()
     hid_in[3] = up_group(3)
-    for m in passed:
-        m.arrived()
-    el_in = expert_up(el, 80, 128)
+    down_group(1)
+
+    second_rows.arrived()
+    el_in = expert_up(el, jnp.concatenate([xo[48:96].astype(BF16), xb[48:96]], axis=0))
     down_group(2)
+    last_rows.arrived()
+    ef_in = expert_up(ef, jnp.concatenate([xl[0], xl[2]], axis=0).astype(BF16))
     down_group(3)
 
     cp_ed.wait()
@@ -513,18 +520,26 @@
             rb[half, r] = blk
             returned.append(Msg(rb.at[half, r], eret.at[me], dev(dz, dy, 0, half)).start())
 
+    def results(ref):
+        return jnp.concatenate([dot(ref[...], ed[...]), jnp.zeros((8, 512), F32)], axis=0)
+
     for m in eh_in:
         m.arrived()
-    eo = dot(eh[...], ed[...])
-    for r in range(9, -1, -1):
+    eo = results(eh)
+    for r in range(7, -1, -1):
         for half in range(2):
-            give_back(half, r, eo[half * 80 + r * 8 : half * 80 + r * 8 + 8])
+            give_back(half, r, eo[half * 48 + r * 6 : half * 48 + r * 6 + 8])
     for m in el_in:
         m.arrived()
-    eo = dot(el[...], ed[...])
-    for r in range(15, 9, -1):
+    eo = results(el)
+    for r in range(14, 7, -1):
         for half in range(2):
-            give_back(half, r, eo[half * 48 + (r - 10) * 8 : half * 48 + (r - 10) * 8 + 8])
+            give_back(half, r, eo[half * 48 + (r - 8) * 6 : half * 48 + (r - 8) * 6 + 8])
+    for m in ef_in:
+        m.arrived()
+    eo = dot(ef[...], ed[...])
+    for half in range(2):
+        give_back(half, 15, eo[half * 8 : half * 8 + 8])
 
     lane = lax.broadcasted_iota(jnp.int32, (48, 512), 1).astype(F32)
     sel = jnp.concatenate(
@@ -596,12 +611,14 @@
             pltpu.VMEM((16, 4, 48, 512), BF16),
             pltpu.VMEM((48, 2048), BF16),
             pltpu.VMEM((768, 512), BF16),
-            pltpu.VMEM((128, 2048), F32),
-            pltpu.VMEM((128, 2048), F32),
-            pltpu.VMEM((128, 2048), BF16),
-            pltpu.VMEM((128, 2048), BF16),
-            pltpu.VMEM((160, 1024), BF16),
+            pltpu.VMEM((96, 2048), F32),
+            pltpu.VMEM((96, 2048), F32),
+            pltpu.VMEM((96, 2048), BF16),
+            pltpu.VMEM((96, 2048), BF16),
+            pltpu.VMEM((3, 8, 2048), F32),
             pltpu.VMEM((96, 1024), BF16),
+            pltpu.VMEM((96, 1024), BF16),
+            pltpu.VMEM((16, 1024), BF16),
             pltpu.VMEM((16, 48, 512), BF16),
             pltpu.VMEM((16, 48, 512), BF16),
             pltpu.VMEM((2, 16, 16, 256), BF16),

time: 59.5 us -> 57.7 us (0.970)
  Pallas kernels: 58.7 us -> 56.9 us
    pallas_call x1, Pallas kernels: 56 us -> 54.2 us  [layer_call(): pl.pallas_call(layer_kernel, out_shape=(jax.ShapeDtypeStruct((48, 512), B...]
where the time goes in v4:
time: 57.7 us; the launch traced here: 57.6 us
  Pallas kernels  56.9 us (99%)
  between operations  0.65 us (1%)
    pallas_call x1, Pallas kernels, layer_call(): pl.pallas_call(layer_kernel, out_shape=(jax.ShapeDtypeStruct((48, 512), B...  54.2 us
    pallas_call x1, Pallas kernels, finish_call(): pl.pallas_call(finish_kernel, out_shape=tuple((jax.ShapeDtypeStruct(a.sha...  2.77 us

profile of v4, /device:TPU:1, one launch (start us, length us, event | category | flops | bytes accessed | tf_op | source)
XLA Modules:
  0.0 57.6 jit_solution(6188928828579022045)
XLA Ops:
  0.6 54.2 %layer.1 = (bf16[48,512]{1,0:T(8,128)(2,1)S(1)}, f32[48,2,128,128]{3,2,1,0:T(8,128)S(1)}, f32[96,128]{1,0:T(8,128)S(1)}, f32[2,48]{1,0:T(2,128)S(1)}) custom-call(bf16[48,2048]{1,0:T(8,128)(2,1)} %tok_h.1, f32[1,2048]{1,0:T(1,128)} %bitcast.22, bf16[2048,256]{1,0:T(8,128)(2,1)} %wq_h.1, bf16[2048,256]{1,0:T(8,128)(2,1)} %wk_h.1, bf16[2048,256]{1,0:T(8,128)(2,1)} %wv_h.1, ...), custom_call_target="tpu_custom_call" | custom-call | tf_op jit(solution)/shard_map/layer/pallas_call | solution.py:568
  54.8 2.8 %finish.1 = (bf16[48,512]{1,0:T(8,128)(2,1)}, f32[48,2,128,128]{3,2,1,0:T(8,128)}, f32[96,128]{1,0:T(8,128)}, f32[2,48]{1,0:T(2,128)}) custom-call(bf16[48,512]{1,0:T(8,128)(2,1)S(1)} %get-tuple-element.12.lay, f32[48,2,128,128]{3,2,1,0:T(8,128)S(1)} %get-tuple-element.13.cell, f32[96,128]{1,0:T(8,128)S(1)} %get-tuple-element.14.norm, ...), custom_call_target="tpu_custom_call" | custom-call | tf_op jit(solution)/shard_map/finish/pallas_call | solution.py:651

commit v5 on v4

--- a/solution.py
+++ b/solution.py
@@ -70,7 +70,7 @@
     wmix_h, gain_h, bg_h, rw_h, gate_h, up_h, down_h, eg_h, eu_h, ed_h,
     out, cell, norm_o, max_o,
     inb, fb, tok, cgain, wts, win, wf, norm, mx, ids, normed, vs, vf, cb, qt, wt, num, wsem, csem, msem,
-    ah, wmix, gain, bg, macc, rw, w, d, eg, eu, ed, meta, g, res, hid, xo, xp, xb, xs, xl, eh, el, ef, sb, rsr, rb, eret,
+    ah, wmix, gain, bg, macc, rw, w, d, eg, eu, ed, meta, g, res, hid, xo, xp, xb, xs, xl, eh, el, sb, rsr, rb, eret,
     ssem, rsem, lsem,
 ):
     me = lax.axis_index("ep")
@@ -116,9 +116,6 @@
     barrier = pltpu.get_barrier_semaphore()
     peers = [dev(0, 0, 1, 0), dev(0, 0, 2, 0), dev(0, 0, 3, 0), dev(0, 0, 0, 1)]
     peers += [dev(dz, dy, 0, 0) for dz, dy in (ZP, ZM, YP, YM, (2, 0), (0, 2))]
-    for peer in peers:
-        pl.semaphore_signal(barrier, inc=1, device_id=peer, device_id_type=MESH)
-
     here = y * 4 + z
     cols = pl.ds(pl.multiple_of(x * 512, 512), 512)
 
@@ -141,6 +138,8 @@
         s = pl.ds(i * CHUNK, CHUNK)
         return pltpu.make_async_copy(cell_h.at[s], cell.at[s], csem.at[i])
 
+    for peer in peers:
+        pl.semaphore_signal(barrier, inc=1, device_id=peer, device_id_type=MESH)
     for cp in small[0:2]:
         cp.wait()
     for i in range(N_CHUNK):
@@ -456,6 +455,9 @@
 
     hid_in[1] = up_group(1)
 
+    pick_group(1)
+    first_rows = pass_rows(0, 48)
+
     t_23.arrived()
     l_22a = spread((2, 3), 0, 1, YP)
     t_21.arrived()
@@ -465,8 +467,9 @@
     u_12.arrived()
     l_22d = spread((1, 2), 3, 1, ZM)
 
-    pick_group(1)
-    first_rows = pass_rows(0, 48)
+    for m in down_p:
+        m.arrived()
+    down_group(0)
     for m in (h_32a, h_32b, h_12a, h_12b, h_23a, h_23b, h_21a, h_21b):
         m.arrived()
     hid_in[2] = up_group(2)
@@ -488,9 +491,6 @@
 
     first_rows.arrived()
     eh_in = expert_up(eh, jnp.concatenate([xo[0:48].astype(BF16), xb[0:48]], axis=0))
-    for m in down_p:
-        m.arrived()
-    down_group(0)
 
     for m in (l_22a, l_22b, l_22c, l_22d):
         m.arrived()
@@ -498,12 +498,11 @@
     last_rows = Msg(xl.at[1], xl.at[2], dev(0, 0, 0, 1)).start()
     hid_in[3] = up_group(3)
     down_group(1)
-
     second_rows.arrived()
-    el_in = expert_up(el, jnp.concatenate([xo[48:96].astype(BF16), xb[48:96]], axis=0))
+    el_in = expert_up(el.at[0:96], jnp.concatenate([xo[48:96].astype(BF16), xb[48:96]], axis=0))
     down_group(2)
     last_rows.arrived()
-    ef_in = expert_up(ef, jnp.concatenate([xl[0], xl[2]], axis=0).astype(BF16))
+    el_in += expert_up(el.at[96:112], jnp.concatenate([xl[0], xl[2]], axis=0).astype(BF16))
     down_group(3)
 
     cp_ed.wait()
@@ -532,15 +531,15 @@
     for m in el_in:
         m.arrived()
     eo = results(el)
+    for half in range(2):
+        give_back(half, 15, eo[96 + half * 8 : 104 + half * 8])
     for r in range(14, 7, -1):
         for half in range(2):
             give_back(half, r, eo[half * 48 + (r - 8) * 6 : half * 48 + (r - 8) * 6 + 8])
-    for m in ef_in:
-        m.arrived()
-    eo = dot(ef[...], ed[...])
-    for half in range(2):
-        give_back(half, 15, eo[half * 8 : half * 8 + 8])
-
+
+    early_sends = len(sent) - 52
+    for cp in sent[:early_sends]:
+        cp.wait_send()
     lane = lax.broadcasted_iota(jnp.int32, (48, 512), 1).astype(F32)
     sel = jnp.concatenate(
         [jnp.where(lane == scol[0:48, ch : ch + 1] + float(hf * 8), 1.0, 0.0) for hf in range(2) for ch in range(2)], axis=0
@@ -558,7 +557,7 @@
         first, second = got[hf * 96 : hf * 96 + 48], got[hf * 96 + 48 : hf * 96 + 96]
         out[:, s] = (base[:, s] + first * rwc[0:48, 0:1] + second * rwc[0:48, 1:2]).astype(BF16)
 
-    for cp in sent:
+    for cp in sent[early_sends:]:
         cp.wait_send()
 
 
@@ -617,8 +616,7 @@
             pltpu.VMEM((96, 2048), BF16),
             pltpu.VMEM((3, 8, 2048), F32),
             pltpu.VMEM((96, 1024), BF16),
-            pltpu.VMEM((96, 1024), BF16),
-            pltpu.VMEM((16, 1024), BF16),
+            pltpu.VMEM((112, 1024), BF16),
             pltpu.VMEM((16, 48, 512), BF16),
             pltpu.VMEM((16, 48, 512), BF16),
             pltpu.VMEM((2, 16, 16, 256), BF16),

time: 57.7 us -> 57.8 us (level)
  no operation moved by 1% of the time
where the time goes in v5:
time: 57.8 us; the launch traced here: 57.7 us
  Pallas kernels  57 us (99%)
  between operations  0.65 us (1%)
    pallas_call x1, Pallas kernels, layer_call(): pl.pallas_call(layer_kernel, out_shape=(jax.ShapeDtypeStruct((48, 512), B...  54.2 us
    pallas_call x1, Pallas kernels, finish_call(): pl.pallas_call(finish_kernel, out_shape=tuple((jax.ShapeDtypeStruct(a.sha...  2.77 us

profile of v5, /device:TPU:1, one launch (start us, length us, event | category | flops | bytes accessed | tf_op | source)
XLA Modules:
  0.0 57.7 jit_solution(7477704381903255913)
XLA Ops:
  0.6 54.2 %layer.1 = (bf16[48,512]{1,0:T(8,128)(2,1)S(1)}, f32[48,2,128,128]{3,2,1,0:T(8,128)S(1)}, f32[96,128]{1,0:T(8,128)S(1)}, f32[2,48]{1,0:T(2,128)S(1)}) custom-call(bf16[48,2048]{1,0:T(8,128)(2,1)} %tok_h.1, f32[1,2048]{1,0:T(1,128)} %bitcast.22, bf16[2048,256]{1,0:T(8,128)(2,1)} %wq_h.1, bf16[2048,256]{1,0:T(8,128)(2,1)} %wk_h.1, bf16[2048,256]{1,0:T(8,128)(2,1)} %wv_h.1, ...), custom_call_target="tpu_custom_call" | custom-call | tf_op jit(solution)/shard_map/layer/pallas_call | solution.py:567
  54.9 2.8 %finish.1 = (bf16[48,512]{1,0:T(8,128)(2,1)}, f32[48,2,128,128]{3,2,1,0:T(8,128)}, f32[96,128]{1,0:T(8,128)}, f32[2,48]{1,0:T(2,128)}) custom-call(bf16[48,512]{1,0:T(8,128)(2,1)S(1)} %get-tuple-element.12.lay, f32[48,2,128,128]{3,2,1,0:T(8,128)S(1)} %get-tuple-element.13.cell, f32[96,128]{1,0:T(8,128)S(1)} %get-tuple-element.14.norm, ...), custom_call_target="tpu_custom_call" | custom-call | tf_op jit(solution)/shard_map/finish/pallas_call | solution.py:649

commit v6 on v5

--- a/solution.py
+++ b/solution.py
@@ -304,8 +304,6 @@
         m.arrived()
     col = pl.ds(y * 4, 4)
     m_y = [Msg(meta.at[col], meta.at[col], dev(0, dy, 0, 0)).start() for dy in (2, 1, 3)]
-    a_yp, a_ym = spread(O, 0, 2, YP), spread(O, 0, 2, YM)
-    b_zp, b_zm = spread(O, 2, 2, ZP), spread(O, 2, 2, ZM)
 
     for dx in (2, 1, 3):
         s = (4 - dx) % 4
@@ -314,6 +312,8 @@
         send_ed(dx)
 
     lax.fori_loop(0, N_CHUNK // 2, write_step, 0)
+    a_yp, a_ym = spread(O, 0, 2, YP), spread(O, 0, 2, YM)
+    b_zp, b_zm = spread(O, 2, 2, ZP), spread(O, 2, 2, ZM)
 
     gate_sum = jnp.zeros((48, 1), F32)
     gate_rows = bg[...].astype(F32)

time: 57.8 us -> 57.7 us (level)
  no operation moved by 1% of the time
where the time goes in v6:
time: 57.7 us; the launch traced here: 57.6 us
  Pallas kernels  57 us (99%)
  between operations  0.65 us (1%)
    pallas_call x1, Pallas kernels, layer_call(): pl.pallas_call(layer_kernel, out_shape=(jax.ShapeDtypeStruct((48, 512), B...  54.2 us
    pallas_call x1, Pallas kernels, finish_call(): pl.pallas_call(finish_kernel, out_shape=tuple((jax.ShapeDtypeStruct(a.sha...  2.77 us

profile of v6, /device:TPU:1, one launch (start us, length us, event | category | flops | bytes accessed | tf_op | source)
XLA Modules:
  0.0 57.6 jit_solution(5838179937108247364)
XLA Ops:
  0.6 54.2 %layer.1 = (bf16[48,512]{1,0:T(8,128)(2,1)S(1)}, f32[48,2,128,128]{3,2,1,0:T(8,128)S(1)}, f32[96,128]{1,0:T(8,128)S(1)}, f32[2,48]{1,0:T(2,128)S(1)}) custom-call(bf16[48,2048]{1,0:T(8,128)(2,1)} %tok_h.1, f32[1,2048]{1,0:T(1,128)} %bitcast.22, bf16[2048,256]{1,0:T(8,128)(2,1)} %wq_h.1, bf16[2048,256]{1,0:T(8,128)(2,1)} %wk_h.1, bf16[2048,256]{1,0:T(8,128)(2,1)} %wv_h.1, ...), custom_call_target="tpu_custom_call" | custom-call | tf_op jit(solution)/shard_map/layer/pallas_call | solution.py:567
  54.9 2.8 %finish.1 = (bf16[48,512]{1,0:T(8,128)(2,1)}, f32[48,2,128,128]{3,2,1,0:T(8,128)}, f32[96,128]{1,0:T(8,128)}, f32[2,48]{1,0:T(2,128)}) custom-call(bf16[48,512]{1,0:T(8,128)(2,1)S(1)} %get-tuple-element.12.lay, f32[48,2,128,128]{3,2,1,0:T(8,128)S(1)} %get-tuple-element.13.cell, f32[96,128]{1,0:T(8,128)S(1)} %get-tuple-element.14.norm, ...), custom_call_target="tpu_custom_call" | custom-call | tf_op jit(solution)/shard_map/finish/pallas_call | solution.py:649
